TPU v7x, 256 devices: a whole 4x4x8 slice. The times are simulated.
256 devices in a mesh: sp: 64 (over z, y, core), tp: 4 (over x).
Axes of the slice: x: 4, y: 4, z: 8, core: 2. Of those that a mesh axis runs over, the one named last changes fastest.
Arguments:
- queries: bfloat16 [32768, 1024], P('sp', 'tp'), may hold values from -6 to 6
- keys: bfloat16 [32768, 1024], P('sp', 'tp'), may hold values from -6 to 6
- values: bfloat16 [32768, 1024], P('sp', 'tp'), may hold values from -6 to 6
- output_gate_logits: bfloat16 [32768, 1024], P('sp', 'tp'), may hold values from -6 to 6
- input_gate_log: float32 [32768, 8], P('sp', 'tp'), may hold values from -5 to 125
- forget_gate_logits: float32 [32768, 8], P('sp', 'tp')
- extra_decay_log: float32 [32768, 8], P('sp', 'tp'), may hold values from -1 to 0
- document: int32 [32768], P('sp'), may hold values from 0 to 31, never falling along the last dimension, each value on 1 to 2048 neighbouring positions
- residual: bfloat16 [32768, 2048], P('sp', 'tp'), may hold values from -16 to 16
- cell_norm_gain: bfloat16 [1024], P('tp'), may hold values from 0.099609375 to 1.8984375
- output_weight: bfloat16 [1024, 2048], P('tp'), may hold values from -0.1875 to 0.1875
- mixer_norm_gain: bfloat16 [2048], P('tp'), may hold values from 0.099609375 to 1.8984375
- up_weight: bfloat16 [2048, 8192], P('sp', 'tp'), may hold values from -0.125 to 0.125
- down_weight: bfloat16 [8192, 2048], P('tp', 'sp'), may hold values from -0.0625 to 0.0625
Outputs:
- layer_out: bfloat16 [32768, 2048], P('sp', 'tp')
All inputs are finite; a program needn't handle non-finite values.
Results may differ from a plain program's by a relative error of at most 0.015.
Values may be sent and summed in bfloat16 or wider, within the bound.
A program may use at most 128 MiB of HBM per device.

v0:
```python
import jax
import jax.numpy as jnp
from jax import lax
from jax.sharding import Mesh
from jax.sharding import PartitionSpec as P

DH = 128
BLOCK = 128
SP = ("sp_0", "sp_1", "sp_2")


NEG = -1e30
EPS = 1e-06


def sent_to_all(value, axis):
    copies = jnp.broadcast_to(value, (lax.axis_size(axis), *value.shape))
    return lax.all_to_all(copies, axis, split_axis=0, concat_axis=0, tiled=True)


def of_everyone(value, axis):
    return sent_to_all(value, axis).sum(axis=0)


def rows_first(arrays, axis, dims):
    turned = [jnp.moveaxis(a, dim, 0) for a, dim in zip(arrays, dims)]
    widths = [t[0].size for t in turned]
    both = jnp.concatenate([t.reshape(-1, w) for t, w in zip(turned, widths)], axis=1)
    whole = lax.all_gather(both, axis, axis=0, tiled=True)
    parts = jnp.split(whole, [sum(widths[:k]) for k in range(1, len(widths))], axis=1)
    return tuple(
        (
            jnp.moveaxis(b.reshape(-1, *t.shape[1:]), 0, dim)
            for b, t, dim in zip(parts, turned, dims)
        )
    )


def nothing_yet(value, identity):
    return jax.tree.map(
        lambda a, e: jnp.broadcast_to(jnp.asarray(e, a.dtype), a.shape), value, identity
    )


def all_in_one(value, axis):
    leaves = jax.tree.leaves(value)
    order = sorted(range(len(leaves)), key=lambda k: -leaves[k].size)
    width = (1, *leaves[order[0]].shape)[-1]
    lines = [
        jnp.pad(leaves[k].reshape(-1), (0, -leaves[k].size % width)).reshape(-1, width)
        for k in order
    ]
    both, at, found = (lax.all_gather(jnp.concatenate(lines), axis), 0, {})
    for k, line in zip(order, lines):
        piece = both[:, at : at + len(line)].reshape(len(both), -1)
        found[k] = piece[:, : leaves[k].size].reshape(-1, *leaves[k].shape)
        at += len(line)
    numbers = iter(range(len(leaves)))
    return jax.tree.map(lambda _: found[next(numbers)], value)


def collected_alike(value, axis):
    leaves, found = (jax.tree.leaves(value), {})
    for leading, a in enumerate(leaves):
        if leading not in found:
            alike = [k for k, b in enumerate(leaves) if b.dtype == a.dtype]
            got = (
                all_in_one([leaves[k] for k in alike], axis)
                if len(alike) > 1
                else [lax.all_gather(a, axis)]
            )
            for k, b in zip(alike, got):
                found[k] = b
    numbers = iter(range(len(leaves)))
    return jax.tree.map(lambda _: found[next(numbers)], value)


def entering(value, axes, combine, identity):
    before = start = nothing_yet(value, identity)
    subtotal = value
    for axis in reversed(axes):
        count, index = (lax.axis_size(axis), lax.axis_index(axis))
        pieces = collected_alike(subtotal, axis)
        inside, subtotal = (start, start)
        for k in range(count):
            passed = k < index
            subtotal = combine(subtotal, jax.tree.map(lambda part: part[k], pieces))
            inside = jax.tree.map(lambda new, old: jnp.where(passed, new, old), subtotal, inside)
        before = combine(inside, before)
    return before


def cut_along(value, dim, count):
    lengths = value.shape
    parts = value.reshape(*lengths[:dim], count, lengths[dim] // count, *lengths[dim + 1 :])
    return jnp.moveaxis(parts, dim, 0)


def summed_on_arrival(value, axis, dim):
    parts = cut_along(value, dim, lax.axis_size(axis))
    arrived = lax.all_to_all(parts, axis, split_axis=0, concat_axis=0, tiled=True)
    return arrived.astype(jnp.float32).sum(axis=0)


def joined_along(parts, dim):
    parts = jnp.moveaxis(parts, 0, dim)
    lengths = parts.shape
    return parts.reshape(*lengths[:dim], lengths[dim] * lengths[dim + 1], *lengths[dim + 2 :])


def gathered_copies(value, axis, dim):
    return joined_along(sent_to_all(value, axis), dim)


def block_terms(carry, inputs):
    memory, normer, stabil, last_doc = carry
    q_blk, k_blk, v_blk, gate_in, gate_log, doc_blk = inputs
    length = doc_blk.shape[0]
    causal = jnp.arange(length)[:, None] >= jnp.arange(length)[None, :]
    cumulative = jnp.cumsum(gate_log, axis=-1)
    same_doc = (doc_blk[:, None] == doc_blk[None, :]) & causal
    pair_log = cumulative[:, :, None] - cumulative[:, None, :] + gate_in[:, None, :]
    pair_log = jnp.where(same_doc[None], pair_log, NEG)
    live_rows = doc_blk == last_doc
    carried_log = jnp.where(live_rows[None, :], cumulative + stabil[:, None], NEG)
    peak_log = jnp.maximum(carried_log, jnp.max(pair_log, axis=-1))
    weights = jnp.exp(pair_log - peak_log[:, :, None])
    carried = jnp.exp(carried_log - peak_log)
    scores = jnp.einsum("htd,hsd->hts", q_blk, k_blk) * weights
    numerator = carried[:, :, None] * jnp.einsum("htd,hde->hte", q_blk, memory)
    numerator = numerator + jnp.einsum("hts,hse->hte", scores, v_blk)
    denominator = carried * jnp.einsum("htd,hd->ht", q_blk, normer) + jnp.sum(scores, axis=-1)
    end_doc = doc_blk[-1]
    end_cum = cumulative[:, -1]
    keep_log = jnp.where(
        (doc_blk == end_doc)[None, :], end_cum[:, None] - cumulative + gate_in, NEG
    )
    old_log = jnp.where(last_doc == end_doc, end_cum + stabil, NEG)
    new_stab = jnp.maximum(old_log, jnp.max(keep_log, axis=-1))
    scaled = jnp.exp(keep_log - new_stab[:, None])
    decayed = jnp.exp(old_log - new_stab)
    memory = decayed[:, None, None] * memory + jnp.einsum("hs,hsd,hse->hde", scaled, k_blk, v_blk)
    normer = decayed[:, None] * normer + jnp.einsum("hs,hsd->hd", scaled, k_blk)
    return ((memory, normer, new_stab, end_doc), (numerator, denominator, peak_log, cumulative))


def split_heads(source, blocks):
    return source.astype(jnp.float32).reshape(blocks, BLOCK, -1, DH).transpose(0, 2, 1, 3)


def split_gates(source, blocks):
    return source.reshape(blocks, BLOCK, -1).transpose(0, 2, 1)


def within_block_pass(
    queries, keys, values, input_gate_log, forget_gate_logits, extra_decay_log, document
):
    blocks = queries.shape[0] // BLOCK
    head_count = queries.shape[1] // DH
    query_heads = split_heads(queries, blocks) * DH ** (-0.5)
    forget_log_values = jax.nn.log_sigmoid(forget_gate_logits) + extra_decay_log
    inputs = (
        query_heads,
        split_heads(keys, blocks),
        split_heads(values, blocks),
        split_gates(input_gate_log, blocks),
        split_gates(forget_log_values, blocks),
        document.reshape(blocks, BLOCK),
    )
    initial = (
        jnp.zeros((head_count, DH, DH), jnp.float32),
        jnp.zeros((head_count, DH), jnp.float32),
        jnp.full((head_count,), NEG, jnp.float32),
        jnp.array(-1, jnp.int32),
    )
    final_state, output_rows = lax.scan(block_terms, initial, inputs)
    return (query_heads, final_state, output_rows)


def head_mix(cell_out, output_gate_logits, cell_norm_gain):
    row_count = output_gate_logits.shape[0]
    head_count = cell_out.shape[1]
    hidden = cell_out.transpose(0, 2, 1, 3).reshape(row_count, head_count * DH)
    squares = of_everyone(jnp.sum(hidden * hidden, axis=1), "tp")
    inverse = lax.rsqrt(squares / (head_count * DH * lax.axis_size("tp")) + EPS)
    gated = jax.nn.sigmoid(output_gate_logits.astype(jnp.float32))
    gains = cell_norm_gain.astype(jnp.float32)
    return (gated * hidden * inverse[:, None] * gains[None, :]).astype(jnp.bfloat16)


def join_states(earlier, later):
    mem_a, norm_a, stab_a, log_a, first_a, last_a = earlier
    mem_b, norm_b, stab_b, log_b, first_b, last_b = later
    joined = last_a == last_b
    stab_ab = jnp.where(joined, jnp.maximum(log_b + stab_a, stab_b), stab_b)
    weight_a = jnp.where(joined, jnp.exp(log_b + stab_a - stab_ab), 0.0)
    weight_b = jnp.exp(stab_b - stab_ab)
    memory = weight_a[:, None, None] * mem_a + weight_b[:, None, None] * mem_b
    normer = weight_a[:, None] * norm_a + weight_b[:, None] * norm_b
    blank_b = last_b < 0
    memory = jnp.where(blank_b, mem_a, memory)
    normer = jnp.where(blank_b, norm_a, normer)
    stabil = jnp.where(blank_b, stab_a, stab_ab)
    first_doc = jnp.where(first_a < 0, first_b, first_a)
    last_doc = jnp.where(blank_b, last_a, last_b)
    return (memory, normer, stabil, log_a + log_b, first_doc, last_doc)


def local(
    queries,
    keys,
    values,
    output_gate_logits,
    input_gate_log,
    forget_gate_logits,
    extra_decay_log,
    document,
    residual,
    cell_norm_gain,
    output_weight,
    mixer_norm_gain,
    up_weight,
    down_weight,
):
    up_whole, down_whole = rows_first((up_weight, down_weight), SP, (0, 1))
    query_heads, final_state, output_rows = within_block_pass(
        queries, keys, values, input_gate_log, forget_gate_logits, extra_decay_log, document
    )
    numerator, denominator, peak_log, cumulative = output_rows
    memory, normer, stabil, last_doc = final_state
    step_logs = cumulative[:, :, -1]
    offsets = jnp.cumsum(step_logs, axis=0) - step_logs
    through = cumulative + offsets[:, :, None]
    summary = (memory, normer, stabil, jnp.sum(step_logs, axis=0), document[0], last_doc)
    identity = (
        jnp.zeros_like(memory),
        jnp.zeros_like(normer),
        jnp.full_like(stabil, NEG),
        jnp.zeros_like(stabil),
        jnp.array(-1, jnp.int32),
        jnp.array(-1, jnp.int32),
    )
    prefix = entering(summary, SP, join_states, identity)
    doc_blocks = document.reshape(-1, BLOCK)
    carried_log = jnp.where(
        (doc_blocks == prefix[5])[:, None, :], through + prefix[2][None, :, None], NEG
    )
    merged_peak = jnp.maximum(peak_log, carried_log)
    own_weight = jnp.exp(peak_log - merged_peak)
    far_weight = jnp.exp(carried_log - merged_peak)
    numerator = own_weight[..., None] * numerator + far_weight[..., None] * jnp.einsum(
        "nhtd,hde->nhte", query_heads, prefix[0]
    )
    denominator = own_weight * denominator + far_weight * jnp.einsum(
        "nhtd,hd->nht", query_heads, prefix[1]
    )
    cell_out = numerator / jnp.maximum(jnp.abs(denominator), 1.0)[..., None]
    mixed = head_mix(cell_out, output_gate_logits, cell_norm_gain)
    head_terms = jnp.dot(mixed, output_weight, preferred_element_type=jnp.float32)
    width = residual.shape[1]
    model_width = width * lax.axis_size("tp")
    own_sum = summed_on_arrival(head_terms.astype(jnp.bfloat16), "tp", 1)
    first_sum = (residual.astype(jnp.float32) + own_sum).astype(jnp.bfloat16)
    first_wide = lax.optimization_barrier(first_sum).astype(jnp.float32)
    squares = of_everyone(jnp.sum(first_wide * first_wide, axis=1), "tp")
    inverse = lax.rsqrt(squares / model_width + EPS)
    normed_own = (first_wide * inverse[:, None] * mixer_norm_gain.astype(jnp.float32)).astype(
        jnp.bfloat16
    )
    normed_full = gathered_copies(normed_own, "tp", 1)
    hidden = jnp.dot(normed_full, up_whole, preferred_element_type=jnp.float32)
    squared = jnp.square(jax.nn.relu(hidden)).astype(jnp.bfloat16)
    channel = jnp.dot(squared, down_whole, preferred_element_type=jnp.float32)
    own_channel = summed_on_arrival(channel.astype(jnp.bfloat16), "tp", 1)
    return (lax.optimization_barrier(first_sum).astype(jnp.float32) + own_channel).astype(
        jnp.bfloat16
    )


def solution(mesh):
    split = Mesh(mesh.devices.reshape(8, 4, 2, mesh.shape["tp"]), ("sp_0", "sp_1", "sp_2", "tp"))
    return jax.shard_map(
        local,
        mesh=split,
        in_specs=(
            P(SP, "tp"),
            P(SP, "tp"),
            P(SP, "tp"),
            P(SP, "tp"),
            P(SP, "tp"),
            P(SP, "tp"),
            P(SP, "tp"),
            P(SP),
            P(SP, "tp"),
            P("tp"),
            P("tp", None),
            P("tp"),
            P(SP, "tp"),
            P("tp", SP),
        ),
        out_specs=P(SP, "tp"),
        check_vma=False,
    )
```

profile of v0, /device:TPU:1, one launch (start us, length us, event | category | flops | bytes accessed | tf_op | source)
XLA Modules:
  0.0 278.6 jit_solution(83311342895520995)
XLA Ops:
  6.7 1.1 convert_multiply_fusion.2
  7.8 1.2 reshape.3525
  9.0 1.0 reshape.3526
  10.6 25.0 %while.25 = (s32[]{:T(128)}, f32[2,128,128]{2,1,0:T(8,128)S(1)}, f32[2,128]{1,0:T(2,128)S(1)}, f32[2]{0:T(128)S(1)}, s32[]{:T(128)}, /*index=5*/f32[4,2,128,128]...) while((s32[]{:T(128)}, f32[2,128,128]{2,1,0:T(8,128)S(1)}, ...), condition=%wide.region_5.6_spmd.clone, body=%wide.region_0.5_spmd.clone.sunk | while | flops 34361868 | bytes 2780512 | solution.py:176
  12.3 0.9 fusion.317
  18.5 0.9 fusion.317
  24.8 0.9 fusion.317
  31.0 0.9 fusion.317
  37.7 4.7 %all-reduce.6 = s32[4]{0:T(128)S(1)} all-reduce(s32[4]{0:T(128)S(1)} %fusion.253), channel_id=2, replica_groups=mesh['sp_0'=8,'sp_1'=4,'sp_2'=2,'tp'=4] {'sp_2'}, use_global_device_ids=true, to_apply=%add.6 | all-reduce | flops 4 | bytes 32
  49.9 5.4 %all-reduce.7 = s32[8]{0:T(128)S(1)} all-reduce(s32[8]{0:T(128)S(1)} %fusion.254), channel_id=3, replica_groups=mesh['sp_0'=8,'sp_1'=4,'sp_2'=2,'tp'=4] {'sp_1'}, use_global_device_ids=true, to_apply=%add.7 | all-reduce | flops 8 | bytes 64
  57.4 4.0 %all-gather.6 = f32[2,260,128]{2,1,0:T(8,128)S(1)} all-gather(f32[1,260,128]{2,1,0:T(8,128)S(1)} %maximum_bitcast_fusion), channel_id=5, replica_groups=mesh['sp_0'=8,'sp_1'=4,'sp_2'=2,'tp'=4] {'sp_2'}, dimensions={0}, use_global_device_ids=true | all-gather | bytes 399360 | tf_op jit(solution)/shard_map/all_gather | solution.py:53
  61.8 9.9 %all-gather.7 = f32[4,260,128]{2,1,0:T(8,128)S(1)} all-gather(f32[1,260,128]{2,1,0:T(8,128)S(1)} %maximum_bitcast_fusion.1), channel_id=6, replica_groups=mesh['sp_0'=8,'sp_1'=4,'sp_2'=2,'tp'=4] {'sp_1'}, dimensions={0}, use_global_device_ids=true | all-gather | bytes 665600 | tf_op jit(solution)/shard_map/all_gather | solution.py:53
  84.4 13.2 %all-reduce.8 = s32[16]{0:T(128)S(1)} all-reduce(s32[16]{0:T(128)S(1)} %fusion.255), channel_id=4, replica_groups=mesh['sp_0'=8,'sp_1'=4,'sp_2'=2,'tp'=4] {'sp_0'}, use_global_device_ids=true, to_apply=%add.8 | all-reduce | flops 16 | bytes 128
  114.1 0.8 copy.162
  115.6 0.8 copy.164
  117.3 1.4 fusion.280
  120.1 0.8 copy.154
  121.4 0.8 fusion.281
  122.5 0.9 add_select_fusion.4
  123.7 2.1 multiply_reduce_fusion
  126.4 3.9 %all-to-all-start = ((f32[4,1,512]{2,1,0:T(1,128)}), f32[4,1,512]{2,1,0:T(1,128)S(1)}, u32[]{:S(2)}, u32[]{:S(2)}) async-start(f32[4,1,512]{2,1,0:T(1,128)} %broadcast_in_dim.110), calls=%async_computation | async-start | bytes 16384 | tf_op jit(solution)/shard_map/all_to_all | solution.py:18
  130.5 3.9 %all-to-all-done = f32[4,1,512]{2,1,0:T(1,128)S(1)} async-done(((f32[4,1,512]{2,1,0:T(1,128)}), f32[4,1,512]{2,1,0:T(1,128)S(1)}, u32[]{:S(2)}, u32[]{:S(2)}) %all-to-all-start) | async-done | bytes 8224 | tf_op jit(solution)/shard_map/all_to_all | solution.py:18
  134.5 1.7 convolution_convert_fusion
  136.4 20.6 %all_to_all.27 = bf16[4,512,512]{2,1,0:T(8,128)(2,1)S(1)} all-to-all(bf16[4,512,512]{2,1,0:T(8,128)(2,1)S(1)} %bitcast.687), channel_id=1, replica_groups=mesh['sp_0'=8,'sp_1'=4,'sp_2'=2,'tp'=4] {'tp'}, dimensions={0} | all-to-all | bytes 4194304 | tf_op jit(solution)/shard_map/all_to_all | solution.py:101
  159.0 3.2 %all-to-all-start.2 = ((f32[4,1,512]{2,1,0:T(1,128)}), f32[4,1,512]{2,1,0:T(1,128)S(1)}, u32[]{:S(2)}, u32[]{:S(2)}) async-start(f32[4,1,512]{2,1,0:T(1,128)} %broadcast_in_dim.111), calls=%async_computation.2 | async-start | bytes 16384 | tf_op jit(solution)/shard_map/all_to_all | solution.py:18
  162.3 4.1 %all-to-all-done.2 = f32[4,1,512]{2,1,0:T(1,128)S(1)} async-done(((f32[4,1,512]{2,1,0:T(1,128)}), f32[4,1,512]{2,1,0:T(1,128)S(1)}, u32[]{:S(2)}, u32[]{:S(2)}) %all-to-all-start.2) | async-done | bytes 8224 | tf_op jit(solution)/shard_map/all_to_all | solution.py:18
  167.1 19.4 %all_to_all.28 = bf16[4,512,512]{1,2,0:T(8,128)(2,1)} all-to-all(bf16[4,512,512]{1,2,0:T(8,128)(2,1)S(1)} %broadcast_in_dim.112), channel_id=1, replica_groups=mesh['sp_0'=8,'sp_1'=4,'sp_2'=2,'tp'=4] {'tp'}, dimensions={0} | all-to-all | bytes 4194304 | tf_op jit(solution)/shard_map/all_to_all | solution.py:18
  186.5 35.9 %all-gather.12.cloned.1.call-done = bf16[2048,4096]{1,0:T(8,128)(2,1)} async-done(((bf16[32,4096]{1,0:T(8,128)(2,1)}), bf16[2048,4096]{1,0:T(8,128)(2,1)}) %all-gather.12.cloned.1.call-update) | async-done | bytes 16777232 | tf_op jit(solution)/shard_map/all_gather | solution.py:29
  222.4 16.6 %fusion.24 = bf16[512,2048]{1,0:T(8,128)(2,1)} fusion(bf16[2048,4096]{1,0:T(8,128)(2,1)} %all-gather.12.cloned.1.call-done, bf16[512,2048]{0,1:T(8,128)(2,1)} %bitcast.691), kind=kOutput, calls=%fused_computation.56 | convolution fusion | flops 8594128896 | bytes 20971520 | tf_op jit(solution)/shard_map/dot_general | solution.py:273
  239.0 1.8 copy.230
  240.8 29.7 %all_to_all.29 = bf16[4,512,512]{2,1,0:T(8,128)(2,1)S(1)} all-to-all(bf16[4,512,512]{2,1,0:T(8,128)(2,1)S(1)} %bitcast.688), channel_id=1, replica_groups=mesh['sp_0'=8,'sp_1'=4,'sp_2'=2,'tp'=4] {'tp'}, dimensions={0} | all-to-all | bytes 4194304 | tf_op jit(solution)/shard_map/all_to_all | solution.py:101
  270.8 1.0 fusion.37
  (222 shorter events, 33.7 us)
Async XLA Ops:
  6.5 127.9 %copy-start = (bf16[256,2048]{1,0:T(8,128)(2,1)S(1)}, bf16[256,2048]{1,0:T(8,128)(2,1)}, u32[]{:S(2)}) copy-start(bf16[256,2048]{1,0:T(8,128)(2,1)} %param.26) | copy-start | bytes 3145732
  6.5 3.5 %copy-start.6 = (s32[512]{0:T(512)S(1)}, s32[512]{0:T(512)}, u32[]{:S(2)}) copy-start(s32[512]{0:T(512)} %param.23) | copy-start | bytes 6148
  6.5 4.0 %copy-start.8 = (f32[512,2]{0,1:T(2,128)S(1)}, f32[512,2]{0,1:T(2,128)}, u32[]{:S(2)}) copy-start(f32[512,2]{0,1:T(2,128)} %param.21) | copy-start | bytes 12292
  6.5 4.0 %copy-start.7 = (f32[512,2]{0,1:T(2,128)S(1)}, f32[512,2]{0,1:T(2,128)}, u32[]{:S(2)}) copy-start(f32[512,2]{0,1:T(2,128)} %param.22) | copy-start | bytes 12292
  6.5 110.7 %all-gather.14.cloned.1.call-start = ((), (), s32[]{:S(2)}) async-start(), calls=%async_computation.6 | async-start | bytes 1216512 | tf_op jit(solution)/shard_map/all_gather | solution.py:53
  10.6 25.1 %copy-start.13 = (u32[256]{0:T(256)S(1)}, u32[256]{0:T(256)}, u32[]{:S(2)}) copy-start(u32[256]{0:T(256)} %constant.114) | copy-start | bytes 3076
  10.6 35.4 %copy-start.12 = (u32[256]{0:T(256)S(1)}, u32[256]{0:T(256)}, u32[]{:S(2)}) copy-start(u32[256]{0:T(256)} %constant.119) | copy-start | bytes 3076
  35.6 42.9 %copy-start.4 = (bf16[2048,32]{0,1:T(8,128)(2,1)S(1)}, bf16[2048,32]{0,1:T(8,128)(2,1)}, u32[]{:S(2)}) copy-start(bf16[2048,32]{0,1:T(8,128)(2,1)} %param.29) | copy-start | bytes 393220
  35.6 42.9 %copy-start.5 = (bf16[32,2048]{1,0:T(8,128)(2,1)S(1)}, bf16[32,2048]{1,0:T(8,128)(2,1)}, u32[]{:S(2)}) copy-start(bf16[32,2048]{1,0:T(8,128)(2,1)} %param.28) | copy-start | bytes 393220
  49.2 33.3 %copy-start.11 = (u32[256]{0:T(256)S(1)}, u32[256]{0:T(256)}, u32[]{:S(2)}) copy-start(u32[256]{0:T(256)} %constant.124) | copy-start | bytes 3076
  78.5 143.9 %all-gather.12.cloned.1.call-start = ((), (), s32[]{:S(2)}) async-start(), calls=%async_computation.5 | async-start | bytes 17039360 | tf_op jit(solution)/shard_map/all_gather | solution.py:29
  119.4 4.3 %copy-start.2 = (f32[2,128,128]{1,2,0:T(8,128)S(1)}, f32[2,128,128]{1,2,0:T(8,128)}, u32[]{:S(2)}) copy-start(f32[2,128,128]{1,2,0:T(8,128)} %copy.162) | copy-start | bytes 393220
  120.1 3.6 %copy-start.3 = (f32[2,128,128]{1,2,0:T(8,128)S(1)}, f32[2,128,128]{1,2,0:T(8,128)}, u32[]{:S(2)}) copy-start(f32[2,128,128]{1,2,0:T(8,128)} %copy.163) | copy-start | bytes 393220
  123.7 6.6 %copy-start.10 = (bf16[256]{0:T(256)(128)(2,1)S(1)}, bf16[256]{0:T(256)(128)(2,1)}, u32[]{:S(2)}) copy-start(bf16[256]{0:T(256)(128)(2,1)} %param.25) | copy-start | bytes 1540
  126.4 8.0 %all-to-all-start = ((f32[4,1,512]{2,1,0:T(1,128)}), f32[4,1,512]{2,1,0:T(1,128)S(1)}, u32[]{:S(2)}, u32[]{:S(2)}) async-start(f32[4,1,512]{2,1,0:T(1,128)} %broadcast_in_dim.110), calls=%async_computation | async-start | bytes 16384 | tf_op jit(solution)/shard_map/all_to_all | solution.py:18
  157.1 1.0 copy-start.1
  158.1 4.2 %copy-start.9 = (bf16[512]{0:T(512)(128)(2,1)S(1)}, bf16[512]{0:T(512)(128)(2,1)}, u32[]{:S(2)}) copy-start(bf16[512]{0:T(512)(128)(2,1)} %param.27) | copy-start | bytes 3076
  159.0 7.4 %all-to-all-start.2 = ((f32[4,1,512]{2,1,0:T(1,128)}), f32[4,1,512]{2,1,0:T(1,128)S(1)}, u32[]{:S(2)}, u32[]{:S(2)}) async-start(f32[4,1,512]{2,1,0:T(1,128)} %broadcast_in_dim.111), calls=%async_computation.2 | async-start | bytes 16384 | tf_op jit(solution)/shard_map/all_to_all | solution.py:18
Sparse Core Ops, SparseCore 0:
  78.6 38.6 all-gather.13
  120.0 102.3 all-gather.11
where the time goes:
time: 280 us; the launch traced here: 279 us
  blocking collectives  107 us (38%)
  between operations  46.7 us (17%)
  waiting for transfers between devices  44.1 us (16%)
  local copies, waits for them, and re-layouts  26.7 us (10%)
  matrix products  25.1 us (9%)
  other arithmetic  17 us (6%)
  starting transfers between devices  7.18 us (3%)
  loops' own time  4.89 us (2%)
    all_to_all x2, blocking collectives, summed_on_arrival(): lax.all_to_all(parts, axis, split_axis=0, concat_axis=0, tiled=True)  50.3 us
    all_gather x1, waiting for transfers between devices, rows_first(): whole = lax.all_gather(both, axis, axis=0, tiled=True)  35.9 us
    unnamed x3, blocking collectives  23.2 us
    all_to_all x1, blocking collectives, sent_to_all(): return lax.all_to_all(copies, axis, split_axis=0, concat_axis=0, tiled=True)  19.4 us
    dot_general x1, matrix products, local(): channel = jnp.dot(squared, down_whole, preferred_element_type=jnp.float32)  16.6 us
    all_gather x2, blocking collectives, all_in_one(): both, at, found = (lax.all_gather(jnp.concatenate(lines), axis), 0, {})  13.9 us
    all_to_all x2, waiting for transfers between devices, sent_to_all(): return lax.all_to_all(copies, axis, split_axis=0, concat_axis=0, tiled=True)  8.02 us
    all_to_all x2, starting transfers between devices, sent_to_all(): return lax.all_to_all(copies, axis, split_axis=0, concat_axis=0, tiled=True)  7.1 us
  transfers between devices with their start and end apart: 4, of which 4 were waited for; matrix products, arithmetic and copies ran while one was open for 7% of the time, Pallas kernels for 0%

commit v1 on v0

v1 whole, which is shorter than its diff:
```python
import jax
import jax.numpy as jnp
from jax import lax
from jax.experimental import pallas as pl
from jax.experimental.pallas import tpu as pltpu
from jax.sharding import Mesh
from jax.sharding import PartitionSpec as P

MESH = pl.DeviceIdType.MESH
SP = ("z", "y", "c")
NZ, NY, NC, NX = 8, 4, 2, 4
ROWS, DH, BLK = 512, 128, 128
HW = 256
DM = 2048
OWN = 512
NB = ROWS // BLK
BACK = 4
NEG = -1e30
EPS = 1e-6
F32, BF16 = jnp.float32, jnp.bfloat16


def rcopy(src, dst, sems, i, dev):
    return pltpu.make_async_remote_copy(
        src_ref=src, dst_ref=dst, send_sem=sems[0].at[i], recv_sem=sems[1].at[i],
        device_id=dev, device_id_type=MESH,
    )


def across(row):
    return jnp.transpose(jnp.broadcast_to(row, (BLK, BLK)))


def rows_of(values):
    return lax.dot_general(
        jnp.ones((8, BLK), F32), values, (((1,), (1,)), ((), ())),
        precision=lax.Precision.HIGHEST, preferred_element_type=F32,
    )


class Gather:
    def __init__(self, view, sems, base, x):
        self.view, self.sems, self.base, self.x = view, sems, base, x
        self.right, self.left = lax.rem(x + 1, NX), lax.rem(x + NX - 1, NX)

    def start(self):
        own = self.view(self.x, None)
        self.r = rcopy(own, own, self.sems, self.base, {"x": self.right})
        self.l = rcopy(own, own, self.sems, self.base + 1, {"x": self.left})
        self.r.start()
        self.l.start()

    def forward(self):
        self.r.wait_recv()
        a = self.view(self.left, 0)
        self.fr = rcopy(a, a, self.sems, self.base + 2, {"x": self.right})
        self.fr.start()
        self.l.wait_recv()
        b = self.view(self.right, 1)
        self.fl = rcopy(b, b, self.sems, self.base + 3, {"x": self.left})
        self.fl.start()

    def finish(self):
        self.fr.wait_recv()
        self.fl.wait_recv()
        for d in (self.r, self.l, self.fr, self.fl):
            d.wait_send()


def kernel(
    small_h, q_h, k_h, v_h, og_h, res_h, wout_h,
    normed, first_own,
    small, q, k, v, og, res, wc, nd, top, stout, auxout, stin, auxin,
    u, line1, line1in, full, line2, line2in,
    lsem, wss, wrs, wds, wdr, sts, strv, gss, grs, lns, lnr,
):
    z, y, c, x = (lax.axis_index(a) for a in ("z", "y", "c", "x"))
    sp = (z * NY + y) * NC + c
    right, left = lax.rem(x + 1, NX), lax.rem(x + NX - 1, NX)

    def at_sp(s):
        s = lax.rem(s + 64, 64)
        return {"z": s // 8, "y": lax.rem(s // 2, NY), "c": lax.rem(s, 2)}

    own_cols = pl.ds(pl.multiple_of(x * OWN, OWN), OWN)
    loads = {}
    for i, (name, src, dst) in enumerate((
        ("small", small_h, small), ("k", k_h, k), ("v", v_h, v), ("q", q_h, q),
        ("og", og_h, og), ("res", res_h, res),
        ("w", wout_h.at[:, own_cols], wc.at[pl.ds(pl.multiple_of(x * HW, HW), HW), :]),
    )):
        loads[name] = pltpu.make_async_copy(src, dst, lsem.at[i])
        loads[name].start()

    barrier = pltpu.get_barrier_semaphore()
    peers = [{"x": lax.rem(x + r, NX)} for r in range(1, NX)]
    peers.append({"c": 1 - c})
    for j in range(1, BACK + 1):
        peers.append(at_sp(sp + j))
        peers.append(at_sp(sp - j))
    for peer in peers:
        pl.semaphore_signal(barrier, inc=1, device_id=peer, device_id_type=MESH)
    pl.semaphore_wait(barrier, len(peers))

    wsend = []
    for r in range(1, NX):
        to = lax.rem(x + r, NX)
        d = rcopy(
            wout_h.at[pl.ds(pl.multiple_of(c * 128, 128), 128), pl.ds(pl.multiple_of(to * OWN, OWN), OWN)],
            wc.at[pl.ds(pl.multiple_of(x * HW + c * 128, 128), 128), :],
            (wss, wrs), r - 1, {"x": to},
        )
        d.start()
        wsend.append(d)

    loads["small"].wait()
    ga = [small[0:8, a * BLK:(a + 1) * BLK] for a in range(NB)]
    lf = jnp.concatenate([small[8:16, a * BLK:(a + 1) * BLK] for a in range(NB)], axis=0)
    ri = lax.broadcasted_iota(jnp.int32, (BLK, BLK), 0)
    ci = lax.broadcasted_iota(jnp.int32, (BLK, BLK), 1)
    upper = (ri <= ci).astype(F32)
    cum = jnp.dot(lf, upper, precision=lax.Precision.HIGHEST, preferred_element_type=F32)
    cm = [cum[8 * a:8 * a + 8] for a in range(NB)]
    tot = [jnp.broadcast_to(cm[a][:, BLK - 1:BLK], (8, BLK)) for a in range(NB)]

    def between(b, a):
        s = jnp.zeros((8, BLK), F32)
        for i in range(b, a):
            s = s + tot[i]
        return s

    ex = [[ga[b] - cm[b] + between(b, a) if a == b else ga[b] + ((tot[b] - cm[b]) + between(b + 1, a))
           for b in range(min(a + 1, NB))] for a in range(NB + 1)]
    doc_last = jnp.broadcast_to(ga[NB - 1][2:3, BLK - 1:BLK], (8, BLK))
    doc_first = jnp.broadcast_to(ga[0][2:3, 0:1], (8, BLK))
    kept = [jnp.where(jnp.broadcast_to(ga[b][2:3], (8, BLK)) == doc_last, ex[NB][b], NEG) for b in range(NB)]
    peak = jnp.maximum(jnp.maximum(kept[0], kept[1]), jnp.maximum(kept[2], kept[3]))
    peak = jnp.broadcast_to(jnp.max(peak, axis=1, keepdims=True), (8, BLK))
    wt = [jnp.exp(kept[b] - peak) for b in range(NB)]
    wrow = jnp.concatenate(wt, axis=1).astype(BF16)

    loads["k"].wait()
    loads["v"].wait()
    sub = lax.broadcasted_iota(jnp.int32, (8, BLK), 0)
    nrm = jnp.zeros((8, BLK), F32)
    for h in range(2):
        hc = slice(h * DH, (h + 1) * DH)
        kh = k[:, hc]
        scaled = jnp.concatenate(
            [v[b * BLK:(b + 1) * BLK, hc].astype(F32) * across(wt[b][h:h + 1]) for b in range(NB)], axis=0
        ).astype(BF16)
        stout[h * DH:(h + 1) * DH, :] = lax.dot_general(
            kh, scaled, (((0,), (0,)), ((), ())), preferred_element_type=F32
        ).astype(BF16)
        nh = jnp.dot(wrow, kh, preferred_element_type=F32)
        nrm = jnp.where(sub == h, nh, nrm)
    auxout[0:8] = jnp.where(sub == 2, doc_last, peak)
    auxout[8:16] = between(0, NB)
    auxout[16:24] = nrm
    sent = []
    for j in range(1, BACK + 1):
        for i, (src, dst) in enumerate(((stout, stin.at[j - 1]), (auxout, auxin.at[j - 1]))):
            d = rcopy(src, dst, (sts, strv), 2 * (j - 1) + i, at_sp(sp + j))
            d.start()
            sent.append(d)

    loads["q"].wait()
    scale = DH ** (-0.5)
    ones = jnp.ones((ROWS, DH), BF16)
    dcol = [across(ga[a][2:3]) for a in range(NB)]
    for h in range(2):
        hc = slice(h * DH, (h + 1) * DH)
        vx = jnp.concatenate([v[:, hc], ones], axis=1)
        for a in range(NB):
            n = (a + 1) * BLK
            qa = q[a * BLK:n, hc]
            sc = lax.dot_general(qa, k[:n, hc], (((1,), (1,)), ((), ())), preferred_element_type=F32)
            es = []
            for b in range(a + 1):
                ok = dcol[a] == ga[b][2:3]
                if b == a:
                    ok = ok & (ci <= ri)
                es.append(jnp.where(ok, ex[a][b][h:h + 1], NEG))
            best = es[0]
            for e in es[1:]:
                best = jnp.maximum(best, e)
            best = jnp.max(best, axis=1, keepdims=True)
            p = jnp.concatenate(
                [(jnp.exp(es[b] - best) * (sc[:, b * BLK:(b + 1) * BLK] * scale)).astype(BF16) for b in range(a + 1)], axis=1
            )
            nd[h, a * BLK:n, :] = jnp.dot(p, vx[:n], preferred_element_type=F32)
            top[h, a * BLK:n, :] = jnp.broadcast_to(best, (BLK, BLK))

    wpass = []
    for r in range(1, NX):
        wsend[r - 1].wait_recv()
        rows = wc.at[pl.ds(pl.multiple_of(lax.rem(x + NX - r, NX) * HW + c * 128, 128), 128), :]
        d = rcopy(rows, rows, (wds, wdr), r - 1, {"c": 1 - c})
        d.start()
        wpass.append(d)

    for d in sent:
        d.wait_recv()
    gone = jnp.zeros((8, BLK), F32)
    logs = []
    for j in range(1, BACK + 1):
        a = auxin[j - 1, 0:8]
        live = (jnp.broadcast_to(a[2:3], (8, BLK)) == doc_first) & (sp >= j)
        logs.append(jnp.where(live, a + gone, NEG))
        gone = gone + auxin[j - 1, 8:16]
    came = jnp.maximum(jnp.maximum(logs[0], logs[1]), jnp.maximum(logs[2], logs[3]))
    part = [jnp.where(lg > 0.5 * NEG, jnp.exp(lg - came), 0.0) for lg in logs]
    nin = jnp.zeros((8, BLK), F32)
    for j in range(BACK):
        nin = nin + part[j] * auxin[j, 16:24]
    memx = []
    for h in range(2):
        m = jnp.zeros((DH, DH), F32)
        for j in range(BACK):
            m = m + part[j][h:h + 1] * stin[j, h * DH:(h + 1) * DH, :].astype(F32)
        memx.append(jnp.concatenate([m, across(nin[h:h + 1])], axis=1).astype(BF16))

    loads["og"].wait()
    ucols = lambda xi: pl.ds(pl.multiple_of(xi * HW, HW), HW)
    for a in range(NB):
        rows = slice(a * BLK, (a + 1) * BLK)
        squares = jnp.zeros((BLK, DH), F32)
        outs = []
        for h in range(2):
            hc = slice(h * DH, (h + 1) * DH)
            qm = jnp.dot(q[rows, hc], memx[h], preferred_element_type=F32) * scale
            far = jnp.where(dcol[a] == doc_first[0:1], (between(0, a) + came)[h:h + 1], NEG)
            near = top[h, rows, :]
            m = jnp.maximum(near, far)
            wn, wf = jnp.exp(near - m), jnp.exp(far - m)
            num = wn * nd[h, rows, :DH] + wf * qm[:, :DH]
            den = wn * nd[h, rows, DH:] + wf * qm[:, DH:]
            cell = num / jnp.maximum(jnp.abs(den), 1.0)
            squares = squares + cell * cell
            gate = jax.nn.sigmoid(og[rows, hc].astype(F32))
            outs.append((gate * cell * ga[h][3:4]).astype(BF16))
        u[rows, ucols(x)] = jnp.concatenate(outs, axis=1)
        line1[:, rows] = rows_of(squares)

    gu = Gather(
        lambda xi, half: u.at[:, ucols(xi)] if half is None else u.at[pl.ds(half * 256, 256), ucols(xi)],
        (gss, grs), 0, x,
    )
    gu.start()
    lsent = []
    for r in range(1, NX):
        d = rcopy(line1, line1in.at[r - 1], (lns, lnr), r - 1, {"x": lax.rem(x + r, NX)})
        d.start()
        lsent.append(d)
    gu.forward()
    for d in lsent:
        d.wait_recv()
    total = line1[...] + line1in[0] + line1in[1] + line1in[2]
    inv = lax.rsqrt(total / (DH * 8) + EPS)
    loads["w"].wait()
    loads["res"].wait()
    for d in wpass:
        d.wait_recv()
    gu.finish()
    for a in range(NB):
        rows = slice(a * BLK, (a + 1) * BLK)
        ic = across(inv[0:1, rows])
        acc = jnp.dot(u[rows, :], wc[...], preferred_element_type=F32)
        squares = jnp.zeros((BLK, BLK), F32)
        outs = []
        for b in range(OWN // BLK):
            cols = slice(b * BLK, (b + 1) * BLK)
            f = (res[rows, cols].astype(F32) + acc[:, cols] * ic).astype(BF16)
            fw = f.astype(F32)
            squares = squares + fw * fw
            outs.append(f)
        f = jnp.concatenate(outs, axis=1)
        full[rows, own_cols] = f
        first_own[rows, :] = f
        line2[:, rows] = rows_of(squares)
    line2[1:2, :] = small[4:5, :]

    fcols = lambda xi: pl.ds(pl.multiple_of(xi * OWN, OWN), OWN)
    gf = Gather(
        lambda xi, half: full.at[:, fcols(xi)] if half is None else full.at[pl.ds(half * 256, 256), fcols(xi)],
        (gss, grs), 4, x,
    )
    gf.start()
    for r in range(1, NX):
        d = rcopy(line2, line2in.at[r - 1], (lns, lnr), NX - 1 + r - 1, {"x": lax.rem(x + r, NX)})
        d.start()
        lsent.append(d)
    gf.forward()
    for d in lsent[NX - 1:]:
        d.wait_recv()
    total = line2[...] + line2in[0] + line2in[1] + line2in[2]
    inv = lax.rsqrt(total / DM + EPS)
    gf.finish()
    icol = [across(inv[0:1, a * BLK:(a + 1) * BLK]) for a in range(NB)]
    for r in range(NX):
        xi = lax.rem(x + NX - r, NX)
        gain = line2[1:2, :] if r == 0 else line2in[r - 1, 1:2, :]
        for a in range(NB):
            rows = slice(a * BLK, (a + 1) * BLK)
            fw = full[rows, fcols(xi)].astype(F32)
            outs = [
                (fw[:, b * BLK:(b + 1) * BLK] * icol[a] * gain[:, b * BLK:(b + 1) * BLK]).astype(BF16)
                for b in range(OWN // BLK)
            ]
            normed[rows, fcols(xi)] = jnp.concatenate(outs, axis=1)
    for d in wsend + wpass + sent + lsent:
        d.wait_send()


def cell_and_norm(small, q, k, v, og, res, wout):
    dma = pltpu.SemaphoreType.DMA
    return pl.pallas_call(
        kernel,
        out_shape=(
            jax.ShapeDtypeStruct((ROWS, DM), BF16),
            jax.ShapeDtypeStruct((ROWS, OWN), BF16),
        ),
        in_specs=[pl.BlockSpec(memory_space=pl.ANY)] * 7,
        out_specs=(pl.BlockSpec(memory_space=pltpu.VMEM),) * 2,
        scratch_shapes=[
            pltpu.VMEM((16, ROWS), F32),
            *[pltpu.VMEM((ROWS, HW), BF16)] * 4,
            pltpu.VMEM((ROWS, OWN), BF16),
            pltpu.VMEM((4 * HW, OWN), BF16),
            pltpu.VMEM((2, ROWS, 2 * DH), F32),
            pltpu.VMEM((2, ROWS, DH), F32),
            pltpu.VMEM((2 * DH, DH), BF16),
            pltpu.VMEM((24, BLK), F32),
            pltpu.VMEM((BACK, 2 * DH, DH), BF16),
            pltpu.VMEM((BACK, 24, BLK), F32),
            pltpu.VMEM((ROWS, 4 * HW), BF16),
            pltpu.VMEM((8, ROWS), F32),
            pltpu.VMEM((3, 8, ROWS), F32),
            pltpu.VMEM((ROWS, DM), BF16),
            pltpu.VMEM((8, ROWS), F32),
            pltpu.VMEM((3, 8, ROWS), F32),
            dma((7,)), dma((3,)), dma((3,)), dma((3,)), dma((3,)),
            dma((8,)), dma((8,)), dma((8,)), dma((8,)), dma((6,)), dma((6,)),
        ],
        compiler_params=pltpu.CompilerParams(
            collective_id=0, has_side_effects=True, vmem_limit_bytes=48 * 2**20
        ),
        cost_estimate=pl.CostEstimate(flops=40_000_000_000, bytes_accessed=2**22, transcendentals=0),
    )(small, q, k, v, og, res, wout)


def small_rows(igate, fgate, extra, document, cgain, mgain):
    f = lambda a: a.astype(F32)
    cg = f(cgain).reshape(2, DH)
    cgrow = jnp.concatenate([cg.reshape(1, 2 * DH), jnp.zeros((1, ROWS - 2 * DH), F32)], axis=1)
    top = jnp.concatenate(
        [igate.T, f(document)[None], cgrow, f(mgain)[None], jnp.zeros((3, ROWS), F32)], axis=0
    )
    lf = (jax.nn.log_sigmoid(fgate) + extra).T
    return jnp.concatenate([top, lf, jnp.zeros((6, ROWS), F32)], axis=0)


def cut_along(value, dim, count):
    lengths = value.shape
    parts = value.reshape(*lengths[:dim], count, lengths[dim] // count, *lengths[dim + 1 :])
    return jnp.moveaxis(parts, dim, 0)


def summed_on_arrival(value, axis, dim):
    parts = cut_along(value, dim, lax.axis_size(axis))
    arrived = lax.all_to_all(parts, axis, split_axis=0, concat_axis=0, tiled=True)
    return arrived.astype(jnp.float32).sum(axis=0)


def local(
    queries, keys, values, output_gate_logits, input_gate_log, forget_gate_logits, extra_decay_log,
    document, residual, cell_norm_gain, output_weight, mixer_norm_gain, up_weight, down_weight,
):
    both = jnp.concatenate([up_weight, down_weight.T], axis=1)
    whole = lax.all_gather(both, SP, axis=0, tiled=True)
    small = small_rows(
        input_gate_log, forget_gate_logits, extra_decay_log, document, cell_norm_gain, mixer_norm_gain
    )
    normed, first = cell_and_norm(
        small, queries, keys, values, output_gate_logits, residual, output_weight
    )
    hidden = jnp.dot(normed, whole[:, :DM], preferred_element_type=F32)
    squared = jnp.square(jax.nn.relu(hidden)).astype(BF16)
    channel = lax.dot_general(squared, whole[:, DM:], (((1,), (1,)), ((), ())), preferred_element_type=F32)
    own = summed_on_arrival(channel.astype(BF16), "x", 1)
    return (first.astype(F32) + own).astype(BF16)


def solution(mesh):
    split = Mesh(mesh.devices.reshape(NZ, NY, NC, NX), ("z", "y", "c", "x"))
    rows, heads = P(SP, "x"), P("x")
    return jax.shard_map(
        local,
        mesh=split,
        in_specs=(
            rows, rows, rows, rows, rows, rows, rows, P(SP), rows, heads, P("x", None), heads, rows, P("x", SP),
        ),
        out_specs=rows,
        check_vma=False,
    )
```

time: 280 us -> 172 us (0.61)
  blocking collectives: 107 us -> 29.7 us
  Pallas kernels: 0 us -> 54.5 us
  between operations: 46.7 us -> 13.4 us
  local copies, waits for them, and re-layouts: 26.7 us -> 9.24 us
  other arithmetic: 17 us -> 5.05 us
  matrix products: 25.1 us -> 15.9 us
  starting transfers between devices: 7.18 us -> 0.01 us
  loops' own time: 4.89 us -> 0 us
    pallas_call x0 -> x1, Pallas kernels: none -> 54.5 us  [cell_and_norm(): pl.pallas_call(kernel, out_shape=(jax.ShapeDtypeStruct((ROWS, DM), BF16),...]
    unnamed x3 -> x0, blocking collectives: 23.2 us -> none
    all_to_all x2 -> x1, blocking collectives: 50.3 us -> 29.7 us  [summed_on_arrival(): lax.all_to_all(parts, axis, split_axis=0, concat_axis=0, tiled=True)]
    all_to_all x1 -> x0, blocking collectives: 19.4 us -> none  [sent_to_all(): return lax.all_to_all(copies, axis, split_axis=0, concat_axis=0, tiled=True)]
    all_gather x2 -> x0, blocking collectives: 13.9 us -> none  [all_in_one(): both, at, found = (lax.all_gather(jnp.concatenate(lines), axis), 0, {})]
    dot_general x28 -> x1, matrix products: 25.1 us -> 15.9 us  [local(): lax.dot_general(squared, whole[:, DM:], (((1,), (1,)), ((), ())), preferr...]
    all_to_all x2 -> x0, waiting for transfers between devices: 8.02 us -> none  [sent_to_all(): return lax.all_to_all(copies, axis, split_axis=0, concat_axis=0, tiled=True)]
    slice x18 -> x0, local copies, waits for them, and re-layouts: 7.76 us -> none  [the longest x6 3.36 us: entering(): subtotal = combine(subtotal, jax.tree.map(lambda part: part[k], pieces))]
  transfers between devices with their start and end apart: 4 -> 1, of which waited for: 4 -> 1; matrix products, arithmetic and copies ran while one was open for 7% -> 2% of each run, Pallas kernels for 0% -> 32%
where the time goes in v1:
time: 172 us
  Pallas kernels  54.5 us (32%)
  waiting for transfers between devices  43.8 us (25%)
  blocking collectives  29.7 us (17%)
  matrix products  15.9 us (9%)
  between operations  13.4 us (8%)
  local copies, waits for them, and re-layouts  9.24 us (5%)
  other arithmetic  5.05 us (3%)
    pallas_call x1, Pallas kernels, cell_and_norm(): pl.pallas_call(kernel, out_shape=(jax.ShapeDtypeStruct((ROWS, DM), BF16),...  54.5 us
    all_gather x1, waiting for transfers between devices, local(): whole = lax.all_gather(both, SP, axis=0, tiled=True)  43.8 us
    all_to_all x1, blocking collectives, summed_on_arrival(): lax.all_to_all(parts, axis, split_axis=0, concat_axis=0, tiled=True)  29.7 us
    dot_general x1, matrix products, local(): lax.dot_general(squared, whole[:, DM:], (((1,), (1,)), ((), ())), preferr...  15.9 us
    unnamed x12, local copies, waits for them, and re-layouts  6.06 us
  transfers between devices with their start and end apart: 1, of which 1 were waited for; matrix products, arithmetic and copies ran while one was open for 2% of the time, Pallas kernels for 32%

profile of v1, /device:TPU:1, one launch (start us, length us, event | category | flops | bytes accessed | tf_op | source)
XLA Modules:
  0.0 171.7 jit_solution(18202214747724003217)
XLA Ops:
  6.5 0.0 all-gather.2.cloned.1.call-start
  6.5 1.7 pad_maximum_fusion
  8.2 0.0 all-gather.2.cloned.1.call-update
  8.2 0.7 reshape_reshape.4
  8.9 0.7 convert_element_type.20
  9.6 0.7 broadcast_in_dim.21
  10.3 0.7 fusion.13
  11.0 0.7 concatenate.13.small_h
  11.8 0.0 copy-start
  11.8 1.2 copy-done
  13.0 0.0 copy-start.1
  13.0 1.0 copy-done.1
  14.0 0.0 copy-start.2
  14.0 0.9 copy-done.2
  15.0 0.0 copy-start.3
  15.0 0.9 copy-done.3
  15.9 0.0 copy-start.4
  15.9 0.9 copy-done.4
  16.9 0.0 copy-start.5
  16.9 0.9 copy-done.5
  17.8 54.5 %shard_map.136 = (bf16[512,2048]{1,0:T(8,128)(2,1)S(1)}, bf16[512,512]{1,0:T(8,128)(2,1)S(1)}) custom-call(f32[16,512]{1,0:T(8,128)S(1)} %concatenate.13.small_h, bf16[512,256]{1,0:T(8,128)(2,1)S(1)} %copy-done.2, bf16[512,256]{1,0:T(8,128)(2,1)S(1)} %copy-done.3, bf16[512,256]{1,0:T(8,128)(2,1)S(1)} %copy-done.4, bf16[512,256]{1,0:T(8,128)(2,1)S(1)} %copy-done.5, ...), custom_call_target="tpu_custom_call" | custom-call | flops 40000000000 | bytes 4194304 | tf_op jit(solution)/shard_map/pallas_call | solution.py:317
  72.4 43.8 %all-gather.2.cloned.1.call-done = bf16[2048,4096]{1,0:T(8,128)(2,1)} async-done(((bf16[32,4096]{1,0:T(8,128)(2,1)}), bf16[2048,4096]{1,0:T(8,128)(2,1)}) %all-gather.2.cloned.1.call-update) | async-done | bytes 16777232 | tf_op jit(solution)/shard_map/all_gather | solution.py:380
  116.2 15.9 %fusion.6 = bf16[512,2048]{1,0:T(8,128)(2,1)} fusion(bf16[2048,4096]{1,0:T(8,128)(2,1)} %all-gather.2.cloned.1.call-done, bf16[512,2048]{1,0:T(8,128)(2,1)S(1)} %get-tuple-element.8), kind=kOutput, calls=%fused_computation.6 | convolution fusion | flops 8594128896 | bytes 20971520 | tf_op jit(solution)/shard_map/dot_general | solution.py:389
  132.1 1.8 %copy.18 = bf16[64,4,8,512]{3,2,0,1:T(8,128)(2,1)S(1)} copy(bf16[64,4,8,512]{3,2,1,0:T(8,128)(2,1)} %bitcast.15) | data formatting | bytes 4194304 | tf_op jit(solution)/shard_map/reshape | solution.py:365
  133.9 29.7 %all_to_all.5 = bf16[4,512,512]{2,1,0:T(8,128)(2,1)S(1)} all-to-all(bf16[4,512,512]{2,1,0:T(8,128)(2,1)S(1)} %bitcast.14), channel_id=1, replica_groups=mesh['z'=8,'y'=4,'c'=2,'x'=4] {'x'}, dimensions={0} | all-to-all | bytes 4194304 | tf_op jit(solution)/shard_map/all_to_all | solution.py:371
  163.6 0.3 convert_reduce_fusion
  163.9 1.0 add_convert_fusion
  (3 shorter events, 0.0 us)
Async XLA Ops:
  6.5 109.6 %all-gather.2.cloned.1.call-start = ((), (), s32[]{:S(2)}) async-start(), calls=%async_computation.1 | async-start | bytes 17039360 | tf_op jit(solution)/shard_map/all_gather | solution.py:380
  11.8 1.2 copy-start
  13.0 1.0 copy-start.1
  14.0 0.9 copy-start.2
  15.0 0.9 copy-start.3
  15.9 0.9 copy-start.4
  16.9 0.9 copy-start.5
Sparse Core Ops, SparseCore 0:
  10.1 106.0 all-gather.1

commit v2 on v1

--- a/solution.py
+++ b/solution.py
@@ -67,12 +67,167 @@
             d.wait_send()
 
 
+class Weights:
+    RIGHT = (0, -2, 2)
+
+    def __init__(self, wup, wdn, us, ds, z, y, c, dirs):
+        self.wup, self.wdn, self.us, self.ds = wup, wdn, us, ds
+        self.z, self.y, self.c = z, y, c
+        self.yr, self.yl, self.zr, self.zl = dirs
+        self.other = {"c": 1 - c}
+        self.un = self.dn = 0
+        self.all = []
+        self.got = {}
+        self.mates = {"up": [], "down": []}
+
+    def zi(self, o):
+        return lax.rem(self.z + NZ + o, NZ)
+
+    def yi(self, o):
+        return lax.rem(self.y + NY + o, NY)
+
+    def send(self, kind, ref, dev, key):
+        sems, i = (self.us, self.un) if kind == "up" else (self.ds, self.dn)
+        if kind == "up":
+            self.un += 1
+        else:
+            self.dn += 1
+        d = rcopy(ref, ref, sems, i, dev)
+        d.start()
+        self.all.append(d)
+        self.got[key] = d
+
+    def up(self, zo, yo):
+        return self.wup.at[self.zi(zo), self.yi(yo), self.c]
+
+    def begin(self):
+        own = self.up(0, 0)
+        self.send("up", own, self.zr, ("uz", -1))
+        self.send("up", own, self.zl, ("uz", 1))
+        own = self.wdn.at[self.z, self.y, self.c]
+        self.send("down", own, self.yr, ("dy", -1))
+        self.send("down", own, self.yl, ("dy", 1))
+
+    def up_y(self, zo):
+        own = self.up(zo, 0)
+        self.send("up", own, self.yr, ("uy", zo, -1))
+        self.send("up", own, self.yl, ("uy", zo, 1))
+
+    def up_z(self, zo):
+        self.got["uz", zo].wait_recv()
+        if -4 < zo < 0:
+            self.send("up", self.up(zo, 0), self.zr, ("uz", zo - 1))
+        elif 0 < zo < 3:
+            self.send("up", self.up(zo, 0), self.zl, ("uz", zo + 1))
+        self.up_y(zo)
+
+    def up_pass(self, zo):
+        self.got["uy", zo, -1].wait_recv()
+        self.got["uy", zo, 1].wait_recv()
+        if zo in self.RIGHT:
+            self.send("up", self.up(zo, -1), self.yr, ("uo", zo))
+        else:
+            self.send("up", self.up(zo, 1), self.yl, ("uo", zo))
+
+    def mate(self, kind, ref):
+        self.send(kind, ref, self.other, (kind, "mate", len(self.mates[kind])))
+        self.mates[kind].append(self.all[-1])
+
+    def up_mate(self, yo):
+        self.mate("up", self.wup.at[:, self.yi(yo), self.c])
+
+    def down_y(self):
+        lo, hi = pl.ds(0, 16), pl.ds(16, 16)
+        self.got["dy", -1].wait_recv()
+        self.send("down", self.wdn.at[self.z, self.yi(-1), self.c, lo], self.yr, ("do", 0))
+        self.got["dy", 1].wait_recv()
+        self.send("down", self.wdn.at[self.z, self.yi(1), self.c, hi], self.yl, ("do", 1))
+
+    def block(self, zo, half):
+        return self.wdn.at[self.zi(zo), pl.ds(2 * half, 2), self.c]
+
+    def down_z(self, zo, side):
+        dev = self.zr if side < 0 else self.zl
+        last = zo == 3 * side
+        for half in (0, 1):
+            if last and half != (0 if side < 0 else 1):
+                continue
+            self.send("down", self.block(zo, half), dev, ("dz", zo + side, half))
+
+    def down_start(self):
+        self.got["do", 0].wait_recv()
+        self.got["do", 1].wait_recv()
+        self.down_z(0, -1)
+        self.down_z(0, 1)
+        self.mate("down", self.wdn.at[self.z, :, self.c])
+
+    def down_step(self, n):
+        for side in (-1, 1):
+            zo = n * side
+            for half in (0, 1):
+                self.got["dz", zo, half].wait_recv()
+            self.down_z(zo, side)
+            self.mate("down", self.wdn.at[self.zi(zo), :, self.c])
+
+    def down_last(self):
+        self.got["dz", -4, 0].wait_recv()
+        self.got["dz", 4, 1].wait_recv()
+        self.mate("down", self.wdn.at[self.zi(4), :, self.c])
+
+    def serve(self, at):
+        if at == "y0":
+            self.up_y(0)
+            self.down_y()
+            self.up_z(-1)
+            self.up_z(1)
+        elif at == "cell0":
+            self.down_start()
+            self.up_z(-2)
+            self.up_z(2)
+        elif at == "cell1":
+            self.up_pass(0)
+        elif at == "u0":
+            self.up_pass(-1)
+            self.up_pass(1)
+            self.up_z(-3)
+            self.up_z(3)
+        elif at == "u1":
+            self.up_pass(-2)
+            self.up_pass(2)
+            self.down_step(1)
+        elif at == "f0":
+            self.up_z(-4)
+            self.up_mate(0)
+            self.up_pass(-3)
+            self.up_pass(3)
+        elif at == "f1":
+            self.down_step(2)
+            self.up_pass(-4)
+            self.up_mate(-1)
+            self.up_mate(1)
+        elif at == "up":
+            for zo in range(-4, 4):
+                self.got["uo", zo].wait_recv()
+            self.up_mate(2)
+            self.down_step(3)
+            for d in self.mates["up"]:
+                d.wait_recv()
+        elif at == "down":
+            self.down_last()
+            for d in self.mates["down"]:
+                d.wait_recv()
+
+    def end(self):
+        for d in self.all:
+            d.wait_send()
+
+
 def kernel(
-    small_h, q_h, k_h, v_h, og_h, res_h, wout_h,
-    normed, first_own,
+    small_h, q_h, k_h, v_h, og_h, res_h, wout_h, up_h, down_h,
+    out,
     small, q, k, v, og, res, wc, nd, top, stout, auxout, stin, auxin,
-    u, line1, line1in, full, line2, line2in,
-    lsem, wss, wrs, wds, wdr, sts, strv, gss, grs, lns, lnr,
+    u, line1, line1in, full, line2, line2in, normed, wup, wdn, squared, terms, parts,
+    lsem, wss, wrs, wds, wdr, sts, strv, gss, grs, lns, lnr, uss, urs, dss, drs, rss, rrs,
 ):
     z, y, c, x = (lax.axis_index(a) for a in ("z", "y", "c", "x"))
     sp = (z * NY + y) * NC + c
@@ -85,6 +240,7 @@
     own_cols = pl.ds(pl.multiple_of(x * OWN, OWN), OWN)
     loads = {}
     for i, (name, src, dst) in enumerate((
+        ("up", up_h, wup.at[z, y, c]), ("down", down_h, wdn.at[z, y, c]),
         ("small", small_h, small), ("k", k_h, k), ("v", v_h, v), ("q", q_h, q),
         ("og", og_h, og), ("res", res_h, res),
         ("w", wout_h.at[:, own_cols], wc.at[pl.ds(pl.multiple_of(x * HW, HW), HW), :]),
@@ -95,12 +251,20 @@
     barrier = pltpu.get_barrier_semaphore()
     peers = [{"x": lax.rem(x + r, NX)} for r in range(1, NX)]
     peers.append({"c": 1 - c})
+    yr, yl, zr, zl = ({"y": lax.rem(y + 1, NY)}, {"y": lax.rem(y + NY - 1, NY)},
+                      {"z": lax.rem(z + 1, NZ)}, {"z": lax.rem(z + NZ - 1, NZ)})
+    peers += [yr, yl, zr, zl]
     for j in range(1, BACK + 1):
         peers.append(at_sp(sp + j))
         peers.append(at_sp(sp - j))
     for peer in peers:
         pl.semaphore_signal(barrier, inc=1, device_id=peer, device_id_type=MESH)
     pl.semaphore_wait(barrier, len(peers))
+
+    ring = Weights(wup, wdn, (uss, urs), (dss, drs), z, y, c, (yr, yl, zr, zl))
+    loads["up"].wait()
+    loads["down"].wait()
+    ring.begin()
 
     wsend = []
     for r in range(1, NX):
@@ -163,6 +327,7 @@
             d = rcopy(src, dst, (sts, strv), 2 * (j - 1) + i, at_sp(sp + j))
             d.start()
             sent.append(d)
+    ring.serve("y0")
 
     loads["q"].wait()
     scale = DH ** (-0.5)
@@ -190,6 +355,7 @@
             )
             nd[h, a * BLK:n, :] = jnp.dot(p, vx[:n], preferred_element_type=F32)
             top[h, a * BLK:n, :] = jnp.broadcast_to(best, (BLK, BLK))
+        ring.serve("cell%d" % h)
 
     wpass = []
     for r in range(1, NX):
@@ -199,6 +365,7 @@
         d.start()
         wpass.append(d)
 
+    ring.serve("pass")
     for d in sent:
         d.wait_recv()
     gone = jnp.zeros((8, BLK), F32)
@@ -252,7 +419,9 @@
         d = rcopy(line1, line1in.at[r - 1], (lns, lnr), r - 1, {"x": lax.rem(x + r, NX)})
         d.start()
         lsent.append(d)
+    ring.serve("u0")
     gu.forward()
+    ring.serve("u1")
     for d in lsent:
         d.wait_recv()
     total = line1[...] + line1in[0] + line1in[1] + line1in[2]
@@ -276,7 +445,6 @@
             outs.append(f)
         f = jnp.concatenate(outs, axis=1)
         full[rows, own_cols] = f
-        first_own[rows, :] = f
         line2[:, rows] = rows_of(squares)
     line2[1:2, :] = small[4:5, :]
 
@@ -290,7 +458,9 @@
         d = rcopy(line2, line2in.at[r - 1], (lns, lnr), NX - 1 + r - 1, {"x": lax.rem(x + r, NX)})
         d.start()
         lsent.append(d)
+    ring.serve("f0")
     gf.forward()
+    ring.serve("f1")
     for d in lsent[NX - 1:]:
         d.wait_recv()
     total = line2[...] + line2in[0] + line2in[1] + line2in[2]
@@ -308,20 +478,61 @@
                 for b in range(OWN // BLK)
             ]
             normed[rows, fcols(xi)] = jnp.concatenate(outs, axis=1)
-    for d in wsend + wpass + sent + lsent:
+
+    ring.serve("up")
+    for t in range(4):
+        cols = slice(t * 512, (t + 1) * 512)
+        hid = jnp.dot(normed[...], wup[:, :, :, :, cols].reshape(DM, 512), preferred_element_type=F32)
+        hid = jnp.maximum(hid, 0.0)
+        squared[:, cols] = (hid * hid).astype(BF16)
+        ring.serve("up%d" % t)
+    ring.serve("down")
+
+    def project(r):
+        to = lax.rem(x + r, NX)
+        w = wdn[pl.ds(2 * to, 2)].reshape(OWN, DM)
+        return lax.dot_general(squared[...], w, (((1,), (1,)), ((), ())), preferred_element_type=F32)
+
+    first, second = slice(0, 256), slice(256, 512)
+    rsem = (rss, rrs)
+    terms[2] = project(2).astype(BF16)
+    i1 = rcopy(terms.at[2, first], parts.at[0], rsem, 0, {"x": right})
+    i2 = rcopy(terms.at[2, second], parts.at[1], rsem, 1, {"x": left})
+    i1.start()
+    i2.start()
+    c1 = project(1)
+    terms[1] = c1.astype(BF16)
+    i3 = rcopy(terms.at[1, second], parts.at[2], rsem, 2, {"x": right})
+    i3.start()
+    c3 = project(3)
+    terms[3] = c3.astype(BF16)
+    i4 = rcopy(terms.at[3, first], parts.at[3], rsem, 3, {"x": left})
+    i4.start()
+    i1.wait_recv()
+    terms[1, first] = (terms[1, first].astype(F32) + parts[0].astype(F32)).astype(BF16)
+    i5 = rcopy(terms.at[1, first], parts.at[4], rsem, 4, {"x": right})
+    i5.start()
+    i2.wait_recv()
+    terms[3, second] = (terms[3, second].astype(F32) + parts[1].astype(F32)).astype(BF16)
+    i6 = rcopy(terms.at[3, second], parts.at[5], rsem, 5, {"x": left})
+    i6.start()
+    mine = project(0) + full[:, own_cols].astype(F32)
+    for d in (i3, i4, i5, i6):
+        d.wait_recv()
+    out[first] = (mine[first] + parts[3].astype(F32) + parts[4].astype(F32)).astype(BF16)
+    out[second] = (mine[second] + parts[2].astype(F32) + parts[5].astype(F32)).astype(BF16)
+    for d in wsend + wpass + sent + lsent + [i1, i2, i3, i4, i5, i6]:
         d.wait_send()
-
-
-def cell_and_norm(small, q, k, v, og, res, wout):
+    ring.end()
+
+
+def layer(small, q, k, v, og, res, wout, up, down):
     dma = pltpu.SemaphoreType.DMA
     return pl.pallas_call(
         kernel,
-        out_shape=(
-            jax.ShapeDtypeStruct((ROWS, DM), BF16),
-            jax.ShapeDtypeStruct((ROWS, OWN), BF16),
-        ),
-        in_specs=[pl.BlockSpec(memory_space=pl.ANY)] * 7,
-        out_specs=(pl.BlockSpec(memory_space=pltpu.VMEM),) * 2,
+        out_shape=jax.ShapeDtypeStruct((ROWS, OWN), BF16),
+        in_specs=[pl.BlockSpec(memory_space=pltpu.HBM)] * 9,
+        out_specs=pl.BlockSpec(memory_space=pltpu.VMEM),
         scratch_shapes=[
             pltpu.VMEM((16, ROWS), F32),
             *[pltpu.VMEM((ROWS, HW), BF16)] * 4,
@@ -339,14 +550,20 @@
             pltpu.VMEM((ROWS, DM), BF16),
             pltpu.VMEM((8, ROWS), F32),
             pltpu.VMEM((3, 8, ROWS), F32),
-            dma((7,)), dma((3,)), dma((3,)), dma((3,)), dma((3,)),
+            pltpu.VMEM((ROWS, DM), BF16),
+            pltpu.VMEM((NZ, NY, NC, 32, DM), BF16),
+            pltpu.VMEM((NZ, NY, NC, 32, DM), BF16),
+            pltpu.VMEM((ROWS, DM), BF16),
+            pltpu.VMEM((4, ROWS, OWN), BF16),
+            pltpu.VMEM((6, ROWS // 2, OWN), BF16),
+            dma((9,)), dma((3,)), dma((3,)), dma((3,)), dma((3,)),
             dma((8,)), dma((8,)), dma((8,)), dma((8,)), dma((6,)), dma((6,)),
+            dma((35,)), dma((35,)), dma((26,)), dma((26,)), dma((6,)), dma((6,)),
         ],
         compiler_params=pltpu.CompilerParams(
-            collective_id=0, has_side_effects=True, vmem_limit_bytes=48 * 2**20
+            collective_id=0, has_side_effects=True, vmem_limit_bytes=62 * 2**20
         ),
-        cost_estimate=pl.CostEstimate(flops=40_000_000_000, bytes_accessed=2**22, transcendentals=0),
-    )(small, q, k, v, og, res, wout)
+    )(small, q, k, v, og, res, wout, up, down)
 
 
 def small_rows(igate, fgate, extra, document, cgain, mgain):
@@ -360,35 +577,16 @@
     return jnp.concatenate([top, lf, jnp.zeros((6, ROWS), F32)], axis=0)
 
 
-def cut_along(value, dim, count):
-    lengths = value.shape
-    parts = value.reshape(*lengths[:dim], count, lengths[dim] // count, *lengths[dim + 1 :])
-    return jnp.moveaxis(parts, dim, 0)
-
-
-def summed_on_arrival(value, axis, dim):
-    parts = cut_along(value, dim, lax.axis_size(axis))
-    arrived = lax.all_to_all(parts, axis, split_axis=0, concat_axis=0, tiled=True)
-    return arrived.astype(jnp.float32).sum(axis=0)
-
-
 def local(
     queries, keys, values, output_gate_logits, input_gate_log, forget_gate_logits, extra_decay_log,
     document, residual, cell_norm_gain, output_weight, mixer_norm_gain, up_weight, down_weight,
 ):
-    both = jnp.concatenate([up_weight, down_weight.T], axis=1)
-    whole = lax.all_gather(both, SP, axis=0, tiled=True)
     small = small_rows(
         input_gate_log, forget_gate_logits, extra_decay_log, document, cell_norm_gain, mixer_norm_gain
     )
-    normed, first = cell_and_norm(
-        small, queries, keys, values, output_gate_logits, residual, output_weight
-    )
-    hidden = jnp.dot(normed, whole[:, :DM], preferred_element_type=F32)
-    squared = jnp.square(jax.nn.relu(hidden)).astype(BF16)
-    channel = lax.dot_general(squared, whole[:, DM:], (((1,), (1,)), ((), ())), preferred_element_type=F32)
-    own = summed_on_arrival(channel.astype(BF16), "x", 1)
-    return (first.astype(F32) + own).astype(BF16)
+    return layer(
+        small, queries, keys, values, output_gate_logits, residual, output_weight, up_weight, down_weight.T
+    )
 
 
 def solution(mesh):

time: 172 us -> 110 us (0.64)
  Pallas kernels: 54.5 us -> 103 us
  waiting for transfers between devices: 43.8 us -> 0 us
  blocking collectives: 29.7 us -> 0 us
  matrix products: 15.9 us -> 0 us
  between operations: 13.4 us -> 0.05 us
  other arithmetic: 5.05 us -> 0.03 us
  local copies, waits for them, and re-layouts: 9.24 us -> 5.83 us
    pallas_call x1, Pallas kernels: 54.5 us -> 103 us  [layer(): pl.pallas_call(kernel, out_shape=jax.ShapeDtypeStruct((ROWS, OWN), BF16),...]
    all_gather x1 -> x0, waiting for transfers between devices: 43.8 us -> none  [local(): whole = lax.all_gather(both, SP, axis=0, tiled=True)]
    all_to_all x1 -> x0, blocking collectives: 29.7 us -> none  [summed_on_arrival(): lax.all_to_all(parts, axis, split_axis=0, concat_axis=0, tiled=True)]
    dot_general x1 -> x0, matrix products: 15.9 us -> none  [local(): lax.dot_general(squared, whole[:, DM:], (((1,), (1,)), ((), ())), preferr...]
    reshape x1 -> x0, local copies, waits for them, and re-layouts: 1.78 us -> none  [cut_along(): value.reshape(*lengths[:dim], count, lengths[dim] // count, *lengths[dim...]
    unnamed x12 -> x13, local copies, waits for them, and re-layouts: 6.06 us -> 4.57 us
  transfers between devices with their start and end apart: 1 -> 0, of which waited for: 1 -> 0; matrix products, arithmetic and copies ran while one was open for 2% -> 0% of each run, Pallas kernels for 32% -> 0%
where the time goes in v2:
time: 110 us; the launch traced here: 109 us
  Pallas kernels  103 us (94%)
  local copies, waits for them, and re-layouts  5.83 us (5%)
    pallas_call x1, Pallas kernels, layer(): pl.pallas_call(kernel, out_shape=jax.ShapeDtypeStruct((ROWS, OWN), BF16),...  103 us
    unnamed x13, local copies, waits for them, and re-layouts  4.57 us

profile of v2, /device:TPU:1, one launch (start us, length us, event | category | flops | bytes accessed | tf_op | source)
XLA Modules:
  0.0 108.9 jit_solution(313159358229777448)
XLA Ops:
  0.0 0.0 copy-start.5
  0.0 0.7 copy-done.5
  0.7 0.0 copy-start.3
  0.7 0.7 copy-done.3
  1.3 0.0 copy-start.4
  1.3 0.0 copy-start.1
  1.3 0.0 copy-start
  1.4 0.7 copy-done.4
  2.0 0.0 copy-done.1
  2.0 0.0 copy-done
  2.1 0.0 copy-start.2
  2.1 0.7 copy-done.2
  2.8 1.2 %concatenate.10.small_h = f32[16,512]{1,0:T(8,128)} concatenate(f32[2,512]{1,0:T(2,128)S(1)} %bitcast.9, f32[1,512]{1,0:T(1,128)S(1)} %bitcast.7, f32[1,512]{1,0:T(1,128)S(1)} %pad_convert_fusion, f32[1,512]{1,0:T(1,128)S(1)} %bitcast.8, f32[3,512]{1,0:T(4,128)S(1)} %broadcast_in_dim.19, f32[2,512]{1,0:T(2,128)S(1)} %fusion.2, f32[6,512]{1,0:T(8,128)S(1)} %broadcast_in_dim.20), dimensions={0} | concatenate | bytes 65536 | tf_op jit(solution)/shard_map/concatenate | solution.py:577
  4.0 103.0 %shard_map.136 = bf16[512,512]{1,0:T(8,128)(2,1)} custom-call(f32[16,512]{1,0:T(8,128)} %concatenate.10.small_h, bf16[512,256]{1,0:T(8,128)(2,1)} %q_h.1, bf16[512,256]{1,0:T(8,128)(2,1)} %k_h.1, bf16[512,256]{1,0:T(8,128)(2,1)} %v_h.1, bf16[512,256]{1,0:T(8,128)(2,1)} %og_h.1, bf16[512,512]{1,0:T(8,128)(2,1)} %res_h.1, bf16[256,2048]{1,0:T(8,128)(2,1)} %wout_h.1, ...), custom_call_target="tpu_custom_call" | custom-call | tf_op jit(solution)/shard_map/pallas_call | solution.py:531
  107.0 1.9 %copy.16 = bf16[512,512]{1,0:T(8,128)(2,1)} copy(bf16[512,512]{1,0:T(8,128)(2,1)} %shard_map.136) | data formatting | bytes 1048576
  (7 shorter events, 0.0 us)
Async XLA Ops:
  0.0 0.7 copy-start.5
  0.7 0.7 copy-start.3
  1.3 0.7 copy-start.4
  1.3 0.7 copy-start.1
  1.3 0.7 copy-start
  2.1 0.7 copy-start.2

commit v3 on v1

v3 whole, which is shorter than its diff:
```python
import jax
import jax.numpy as jnp
from jax import lax
from jax.experimental import pallas as pl
from jax.experimental.pallas import tpu as pltpu
from jax.sharding import Mesh
from jax.sharding import PartitionSpec as P

MESH = pl.DeviceIdType.MESH
SP = ("z", "y", "c")
NZ, NY, NC, NX = 8, 4, 2, 4
ROWS, DH, BLK = 512, 128, 128
HW = 256
DM = 2048
OWN = 512
NB = ROWS // BLK
NEG = -1e30
EPS = 1e-6
F32, BF16 = jnp.float32, jnp.bfloat16
OFFS = (0, -1, 1, 2)
LOADS = ("up", "down", "ig", "fg", "ex", "doc", "k", "v", "q", "cg", "og", "mg", "res", "w")

RIGHT = (0, -1, 2)

ORDER = (
    "begin", "gates", "state", "dz0,0", "wsend", "uz-1", "dy-1", "uz1", "dy1",
    "st0", "y0", "uyz-1", "dz0,-1", "intra0", "uyz1", "do", "dz0,2", "st1",
    "uz-2", "uz2", "uyz2", "intra1", "dz0,1", "cell", "dz-1,0", "ps1", "ufl",
    "ufr", "uz-3", "uz3", "dz-1,2", "wpass", "uyz-3", "uyz3", "dz1,2", "dz-1,-1",
    "dz1,1", "dz-1,1", "dm-1", "uyz-2", "dz1,-1", "outa", "dz1,0", "uz-4", "outb",
    "ps-3", "dz-2,0", "dz2,-1", "dz2,2", "uyz-4", "dz-2,-1", "ps2", "ps3", "dz-2,1",
    "ps-1", "ps0", "ps-2", "dm0", "ffr", "dz2,1", "dz-2,2", "dz2,0", "ps-4",
    "ffl", "um0", "um-1", "um1", "dm2", "dz3,2", "dz3,1", "dm-2", "dz-3,0",
    "dz-3,-1", "um2", "dz3,0", "dz3,-1", "norm", "up0", "dz4,1", "dz4,2", "dm3",
    "dz-3,1", "dz-3,2", "dm1", "dm-3", "up1", "up2", "dz-4,0", "dz-4,-1", "dm4",
    "up3", "down",
)


def across(row):
    return jnp.transpose(jnp.broadcast_to(row, (BLK, BLK)))


def rows_of(values):
    return lax.dot_general(
        jnp.ones((8, BLK), F32), values, (((1,), (1,)), ((), ())),
        precision=lax.Precision.HIGHEST, preferred_element_type=F32,
    )


def kernel(
    ig_h, fg_h, ex_h, doc_h, cg_h, mg_h, q_h, k_h, v_h, og_h, res_h, wout_h, up_h, down_h,
    out,
    ig, fg, ex, doc, cg, mg, q, k, v, og, res, wc, nd, top, stin, auxin,
    u, line1, line1in, full, line2, line2in, normed, wup, wdn, squared, terms, parts,
    lsem, xss, xrs, sts, strs, uss, urs, dss, drs,
):
    z, y, c, x = (lax.axis_index(a) for a in ("z", "y", "c", "x"))
    chip = z * NY + y

    def at_chip(i):
        i = lax.rem(i + NZ * NY, NZ * NY)
        return {"z": i // NY, "y": lax.rem(i, NY)}

    xi = lambda o: lax.rem(x + NX + o, NX)
    yi = lambda o: lax.rem(y + NY + o, NY)
    zi = lambda o: lax.rem(z + NZ + o, NZ)
    xr, xl, yr, yl, zr, zl = ({a: f(o)} for a, f in (("x", xi), ("y", yi), ("z", zi)) for o in (1, -1))
    mate = {"c": 1 - c}
    ahead, behind = at_chip(chip + 1), at_chip(chip - 1)
    sp = chip * NC + c

    own_cols = pl.ds(pl.multiple_of(x * OWN, OWN), OWN)
    sources = dict(
        up=(up_h, wup.at[z, y, c]), down=(down_h, wdn.at[z, y, c]), ig=(ig_h, ig), fg=(fg_h, fg), ex=(ex_h, ex),
        doc=(doc_h, doc), k=(k_h, k), v=(v_h, v), q=(q_h, q), cg=(cg_h, cg), og=(og_h, og), mg=(mg_h, mg),
        res=(res_h, res), w=(wout_h.at[:, own_cols], wc.at[pl.ds(pl.multiple_of(x * HW, HW), HW), :]),
    )
    loads = {}
    for i, name in enumerate(LOADS):
        loads[name] = pltpu.make_async_copy(*sources[name], lsem.at[i])
        loads[name].start()

    barrier = pltpu.get_barrier_semaphore()
    peers = [xr, xl, {"x": xi(2)}, mate, yr, yl, zr, zl, ahead, behind]
    for peer in peers:
        pl.semaphore_signal(barrier, inc=1, device_id=peer, device_id_type=MESH)
    pl.semaphore_wait(barrier, len(peers))

    pools = {"x": [xss, xrs, 0], "s": [sts, strs, 0], "u": [uss, urs, 0], "d": [dss, drs, 0]}
    copies = {}

    def send(pool, name, src, dst, dev):
        p = pools[pool]
        d = pltpu.make_async_remote_copy(
            src_ref=src, dst_ref=dst, send_sem=p[0].at[p[2]], recv_sem=p[1].at[p[2]],
            device_id=dev, device_id_type=MESH,
        )
        p[2] += 1
        d.start()
        copies[name] = d

    def arrived(*names):
        for name in names:
            copies[name].wait_recv()

    got = {}
    steps = {}

    def step(f):
        steps[f.__name__] = f
        return f

    def up_at(zo, yo):
        return wup.at[zi(zo), yi(yo), c]

    def down_at(zo, yo):
        return wdn.at[zi(zo), yi(yo), c]

    @step
    def begin():
        loads["up"].wait()
        loads["down"].wait()
        own, dn = up_at(0, 0), down_at(0, 0)
        send("u", "uz-1", own, own, zr)
        send("u", "uz1", own, own, zl)
        send("d", "dy-1", dn, dn, yr)
        send("d", "dy1", dn, dn, yl)

    def uz(zo):
        arrived("uz%d" % zo)
        ref = up_at(zo, 0)
        if -4 < zo < 0:
            send("u", "uz%d" % (zo - 1), ref, ref, zr)
        elif 0 < zo < 3:
            send("u", "uz%d" % (zo + 1), ref, ref, zl)

    def uyz(zo):
        ref = up_at(zo, 0)
        send("u", "uy%d,-1" % zo, ref, ref, yr)
        send("u", "uy%d,1" % zo, ref, ref, yl)

    def ps(zo):
        side = -1 if zo in RIGHT else 1
        arrived("uy%d,%d" % (zo, side))
        ref = up_at(zo, side)
        send("u", "uo%d" % zo, ref, ref, yr if side < 0 else yl)

    def um(yo):
        if yo in (-1, 1):
            arrived(*("uy%d,%d" % (zo, yo) for zo in range(-4, 4) if (zo in RIGHT) != (yo == -1)))
        elif yo == 2:
            arrived(*("uo%d" % zo for zo in range(-4, 4)))
        ref = wup.at[:, yi(yo), c]
        send("u", "umr%d" % yo, ref, ref, mate)

    def dy(side):
        arrived("dy%d" % side)
        ref = wdn.at[z, yi(side), c, pl.ds(0 if side < 0 else 16, 16)]
        send("d", "do%d" % side, ref, ref, yr if side < 0 else yl)

    @step
    def do():
        arrived("do-1", "do1")

    def dz(zo, yo):
        ref = down_at(zo, yo)
        if zo:
            arrived("dz%d,%d" % (zo, yo))
        for side, dev, last in ((-1, zr, (0, -1)), (1, zl, (1, 2))):
            if zo * side < 0 or abs(zo) == 4 or (abs(zo) == 3 and yo not in last):
                continue
            send("d", "dz%d,%d" % (zo + side, yo), ref, ref, dev)

    def dm(zo):
        ref = wdn.at[zi(zo), :, c]
        send("d", "dmr%d" % zo, ref, ref, mate)

    for zo in range(-4, 4):
        steps["uz%d" % zo] = lambda zo=zo: uz(zo)
        steps["uyz%d" % zo] = lambda zo=zo: uyz(zo)
        steps["ps%d" % zo] = lambda zo=zo: ps(zo)
    steps["y0"] = steps["uyz0"]
    for o in OFFS:
        steps["um%d" % o] = lambda o=o: um(o)
    for side in (-1, 1):
        steps["dy%d" % side] = lambda side=side: dy(side)
    for zo in range(-4, 5):
        steps["dm%d" % zo] = lambda zo=zo: dm(zo)
        for yo in OFFS:
            steps["dz%d,%d" % (zo, yo)] = lambda zo=zo, yo=yo: dz(zo, yo)

    half = pl.multiple_of(c * 128, 128)
    wrows = lambda o: wc.at[pl.ds(pl.multiple_of(xi(o) * HW + half, 128), 128), :]

    @step
    def wsend():
        for r in range(1, NX):
            cols = pl.ds(pl.multiple_of(xi(r) * OWN, OWN), OWN)
            send("x", "w%d" % r, wout_h.at[pl.ds(half, 128), cols], wrows(0), {"x": xi(r)})

    @step
    def wpass():
        for r in range(1, NX):
            arrived("w%d" % r)
            send("x", "wm%d" % r, wrows(-r), wrows(-r), mate)

    ri = lax.broadcasted_iota(jnp.int32, (BLK, BLK), 0)
    ci = lax.broadcasted_iota(jnp.int32, (BLK, BLK), 1)
    scale = DH ** (-0.5)
    block = lambda a: slice(a * BLK, (a + 1) * BLK)
    head = lambda h: slice(h * DH, (h + 1) * DH)

    @step
    def gates():
        for name in ("ig", "fg", "ex", "doc"):
            loads[name].wait()
        f = fg[...]
        lf = jnp.minimum(f, 0.0) - jnp.log1p(jnp.exp(-jnp.abs(f))) + ex[...]
        docs = doc[...].astype(F32)
        dr = [docs[:, block(a)] for a in range(NB)]
        ga = [ig[:, block(a)] for a in range(NB)]
        cum = jnp.dot(
            jnp.concatenate([lf[:, block(a)] for a in range(NB)], axis=0), (ri <= ci).astype(F32),
            precision=lax.Precision.HIGHEST, preferred_element_type=F32,
        )
        cm = [cum[2 * a:2 * a + 2] for a in range(NB)]
        tot = [jnp.broadcast_to(cm[a][:, BLK - 1:BLK], (2, BLK)) for a in range(NB)]

        def between(b, a):
            s = jnp.zeros((2, BLK), F32)
            for i in range(b, a):
                s = s + tot[i]
            return s

        got.update(
            between=between, dr=dr,
            ex=[[ga[b] - cm[b] if a == b else ga[b] + ((tot[b] - cm[b]) + between(b + 1, a))
                 for b in range(min(a + 1, NB))] for a in range(NB + 1)],
            first=jnp.broadcast_to(dr[0][:, 0:1], (1, BLK)), last=jnp.broadcast_to(dr[NB - 1][:, BLK - 1:BLK], (1, BLK)),
        )
        got["dcol"] = [across(d) for d in dr]

    @step
    def state():
        e = got["ex"][NB]
        kept = [jnp.where(got["dr"][b] == got["last"], e[b], NEG) for b in range(NB)]
        peak = jnp.maximum(jnp.maximum(kept[0], kept[1]), jnp.maximum(kept[2], kept[3]))
        peak = jnp.broadcast_to(jnp.max(peak, axis=1, keepdims=True), (2, BLK))
        wt = [jnp.exp(kept[b] - peak) for b in range(NB)]
        wrow = jnp.concatenate(wt, axis=1)
        loads["k"].wait()
        loads["v"].wait()
        for h in range(2):
            kh = k[:, head(h)]
            scaled = jnp.concatenate(
                [v[block(b), head(h)].astype(F32) * across(wt[b][h:h + 1]) for b in range(NB)], axis=0
            ).astype(BF16)
            stin[5, head(h), :] = lax.dot_general(
                kh, scaled, (((0,), (0,)), ((), ())), preferred_element_type=F32
            ).astype(BF16)
            w8 = jnp.broadcast_to(wrow[h:h + 1], (8, ROWS)).astype(BF16)
            auxin[5, 4 + h:5 + h] = jnp.dot(w8, kh, preferred_element_type=F32)[0:1]
        auxin[5, 0:2] = peak
        auxin[5, 2:4] = got["between"](0, NB)
        auxin[5, 6:7] = got["last"]
        auxin[5, 7:8] = got["last"]
        pass_state(5, 0, ahead)
        pass_state(5, 4, mate)

    def pass_state(slot, to, dev):
        send("s", "st%d" % to, stin.at[slot], stin.at[to], dev)
        send("s", "sx%d" % to, auxin.at[slot], auxin.at[to], dev)

    @step
    def st0():
        arrived("st0", "sx0")
        pass_state(0, 1, ahead)
        pass_state(0, 2, mate)

    @step
    def st1():
        arrived("st1", "sx1")
        pass_state(1, 3, mate)

    def intra(h):
        loads["q"].wait() if h == 0 else None
        vx = jnp.concatenate([v[:, head(h)], jnp.ones((ROWS, DH), BF16)], axis=1)
        for a in range(NB):
            n = (a + 1) * BLK
            sc = lax.dot_general(
                q[block(a), head(h)], k[:n, head(h)], (((1,), (1,)), ((), ())), preferred_element_type=F32
            )
            es = []
            for b in range(a + 1):
                ok = got["dcol"][a] == got["dr"][b]
                if b == a:
                    ok = ok & (ci <= ri)
                es.append(jnp.where(ok, got["ex"][a][b][h:h + 1], NEG))
            best = es[0]
            for e in es[1:]:
                best = jnp.maximum(best, e)
            best = jnp.max(best, axis=1, keepdims=True)
            p = jnp.concatenate(
                [(jnp.exp(es[b] - best) * (sc[:, block(b)] * scale)).astype(BF16) for b in range(a + 1)], axis=1
            )
            nd[h, block(a), :] = jnp.dot(p, vx[:n], preferred_element_type=F32)
            top[h, block(a), :] = jnp.broadcast_to(best, (BLK, BLK))

    steps["intra0"] = lambda: intra(0)
    steps["intra1"] = lambda: intra(1)

    ucols = lambda o: pl.ds(pl.multiple_of(xi(o) * HW, HW), HW)
    uview = lambda o, s: u.at[pl.ds(256 * s, 256), ucols(o)]
    fcols = lambda o: pl.ds(pl.multiple_of(xi(o) * OWN, OWN), OWN)
    fview = lambda o, s: full.at[pl.ds(256 * s, 256), fcols(o)]

    @step
    def cell():
        arrived("st2", "sx2", "st3", "sx3", "st4", "sx4")
        gone = jnp.zeros((2, BLK), F32)
        logs, slots = [], (2 + 2 * c, 0, 3 - c, 1)
        for j, s in enumerate(slots):
            live = (auxin[s, 6:7] == got["first"]) & (sp > j)
            logs.append(jnp.where(live, auxin[s, 0:2] + gone, NEG))
            gone = gone + auxin[s, 2:4]
        came = jnp.maximum(jnp.maximum(logs[0], logs[1]), jnp.maximum(logs[2], logs[3]))
        part = [jnp.where(lg > 0.5 * NEG, jnp.exp(lg - came), 0.0) for lg in logs]
        memx = []
        for h in range(2):
            m, n = jnp.zeros((DH, DH), F32), jnp.zeros((1, BLK), F32)
            for g, s in zip(part, slots):
                m = m + g[h:h + 1] * stin[s, head(h), :].astype(F32)
                n = n + g[h:h + 1] * auxin[s, 4 + h:5 + h]
            memx.append(jnp.concatenate([m, across(n)], axis=1).astype(BF16))
        loads["og"].wait()
        loads["cg"].wait()
        gain = cg[...].astype(F32).reshape(1, HW)
        for a in range(NB):
            squares = jnp.zeros((BLK, DH), F32)
            outs = []
            for h in range(2):
                qm = jnp.dot(q[block(a), head(h)], memx[h], preferred_element_type=F32) * scale
                far = jnp.where(got["dcol"][a] == got["first"], (got["between"](0, a) + came)[h:h + 1], NEG)
                near = top[h, block(a), :]
                m = jnp.maximum(near, far)
                wn, wf = jnp.exp(near - m), jnp.exp(far - m)
                num = wn * nd[h, block(a), :DH] + wf * qm[:, :DH]
                den = wn * nd[h, block(a), DH:] + wf * qm[:, DH:]
                val = num / jnp.maximum(jnp.abs(den), 1.0)
                squares = squares + val * val
                gate = jax.nn.sigmoid(og[block(a), head(h)].astype(F32))
                outs.append((gate * val * gain[:, head(h)]).astype(BF16))
            u[block(a), ucols(0)] = jnp.concatenate(outs, axis=1)
            line1[:, block(a)] = rows_of(squares)
        send("x", "ua-", uview(0, 0), uview(0, 0), xr)
        send("x", "ub+", uview(0, 1), uview(0, 1), xl)
        for r in range(1, NX):
            send("x", "l%d" % r, line1, line1in.at[r - 1], {"x": xi(r)})
        send("x", "ub-", uview(0, 1), uview(0, 1), xr)
        send("x", "ua+", uview(0, 0), uview(0, 0), xl)

    @step
    def ufr():
        arrived("ua-")
        send("x", "uar", uview(-1, 0), uview(-1, 0), xr)

    @step
    def ufl():
        arrived("ub+")
        send("x", "ubl", uview(1, 1), uview(1, 1), xl)

    def project_out(s):
        for a in (2 * s, 2 * s + 1):
            ic = across(got["inv1"][0:1, block(a)])
            acc = jnp.dot(u[block(a), :], wc[...], preferred_element_type=F32)
            squares = jnp.zeros((BLK, BLK), F32)
            outs = []
            for b in range(OWN // BLK):
                f = (res[block(a), block(b)].astype(F32) + acc[:, block(b)] * ic).astype(BF16)
                fw = f.astype(F32)
                squares = squares + fw * fw
                outs.append(f)
            full[block(a), fcols(0)] = jnp.concatenate(outs, axis=1)
            line2[:, block(a)] = rows_of(squares)

    @step
    def outa():
        arrived("l1", "l2", "l3")
        total = line1[...] + line1in[0] + line1in[1] + line1in[2]
        got["inv1"] = lax.rsqrt(total / (DH * 8) + EPS)
        loads["w"].wait()
        loads["res"].wait()
        arrived("wm1", "wm2", "wm3", "ub-", "ua+", "uar", "ubl")
        project_out(0)
        send("x", "fa-", fview(0, 0), fview(0, 0), xr)
        send("x", "fa+", fview(0, 0), fview(0, 0), xl)

    @step
    def outb():
        project_out(1)
        loads["mg"].wait()
        line2[1:2, :] = mg[...].astype(F32).reshape(1, OWN)
        for r in range(1, NX):
            send("x", "m%d" % r, line2, line2in.at[r - 1], {"x": xi(r)})
        send("x", "fb-", fview(0, 1), fview(0, 1), xr)
        send("x", "fb+", fview(0, 1), fview(0, 1), xl)

    @step
    def ffr():
        arrived("fa-")
        send("x", "far", fview(-1, 0), fview(-1, 0), xr)

    @step
    def ffl():
        arrived("fb+")
        send("x", "fbl", fview(1, 1), fview(1, 1), xl)

    @step
    def norm():
        arrived("m1", "m2", "m3")
        total = line2[...] + line2in[0] + line2in[1] + line2in[2]
        inv = lax.rsqrt(total / DM + EPS)
        arrived("fb-", "fa+", "far", "fbl")
        icol = [across(inv[0:1, block(a)]) for a in range(NB)]
        for r in range(NX):
            gain = line2[1:2, :] if r == 0 else line2in[r - 1, 1:2, :]
            for a in range(NB):
                fw = full[block(a), fcols(-r)].astype(F32)
                normed[block(a), fcols(-r)] = jnp.concatenate(
                    [(fw[:, block(b)] * icol[a] * gain[:, block(b)]).astype(BF16) for b in range(OWN // BLK)], axis=1
                )

    def up(t):
        if t == 0:
            arrived("umr0", "umr-1", "umr1", "umr2")
        cols = slice(t * 512, (t + 1) * 512)
        hid = jnp.dot(normed[...], wup[:, :, :, :, cols].reshape(DM, 512), preferred_element_type=F32)
        hid = jnp.maximum(hid, 0.0)
        squared[:, cols] = (hid * hid).astype(BF16)

    for t in range(4):
        steps["up%d" % t] = lambda t=t: up(t)

    @step
    def down():
        arrived(*("dmr%d" % zo for zo in range(-3, 5)))

        def project(r):
            w = wdn[pl.ds(2 * xi(r), 2)].reshape(OWN, DM)
            return lax.dot_general(squared[...], w, (((1,), (1,)), ((), ())), preferred_element_type=F32)

        a, b = slice(0, 256), slice(256, 512)
        terms[2] = project(2).astype(BF16)
        send("x", "p0", terms.at[2, a], parts.at[0], xr)
        send("x", "p1", terms.at[2, b], parts.at[1], xl)
        terms[1] = project(1).astype(BF16)
        send("x", "p2", terms.at[1, b], parts.at[2], xr)
        terms[3] = project(3).astype(BF16)
        send("x", "p3", terms.at[3, a], parts.at[3], xl)
        arrived("p0")
        terms[1, a] = (terms[1, a].astype(F32) + parts[0].astype(F32)).astype(BF16)
        send("x", "p4", terms.at[1, a], parts.at[4], xr)
        arrived("p1")
        terms[3, b] = (terms[3, b].astype(F32) + parts[1].astype(F32)).astype(BF16)
        send("x", "p5", terms.at[3, b], parts.at[5], xl)
        mine = project(0) + full[:, fcols(0)].astype(F32)
        arrived("p2", "p3", "p4", "p5")
        out[a] = (mine[a] + parts[3].astype(F32) + parts[4].astype(F32)).astype(BF16)
        out[b] = (mine[b] + parts[2].astype(F32) + parts[5].astype(F32)).astype(BF16)

    for name in ORDER:
        steps[name]()
    for d in copies.values():
        d.wait_send()


def layer(*arrays):
    dma = pltpu.SemaphoreType.DMA
    return pl.pallas_call(
        kernel,
        out_shape=jax.ShapeDtypeStruct((ROWS, OWN), BF16),
        in_specs=[pl.BlockSpec(memory_space=pltpu.HBM)] * len(arrays),
        out_specs=pl.BlockSpec(memory_space=pltpu.VMEM),
        scratch_shapes=[
            *[pltpu.VMEM(a.shape, a.dtype) for a in arrays[:11]],
            pltpu.VMEM((4 * HW, OWN), BF16),
            pltpu.VMEM((2, ROWS, 2 * DH), F32),
            pltpu.VMEM((2, ROWS, DH), F32),
            pltpu.VMEM((6, 2 * DH, DH), BF16),
            pltpu.VMEM((6, 8, BLK), F32),
            pltpu.VMEM((ROWS, 4 * HW), BF16),
            pltpu.VMEM((8, ROWS), F32),
            pltpu.VMEM((3, 8, ROWS), F32),
            pltpu.VMEM((ROWS, DM), BF16),
            pltpu.VMEM((8, ROWS), F32),
            pltpu.VMEM((3, 8, ROWS), F32),
            pltpu.VMEM((ROWS, DM), BF16),
            pltpu.VMEM((NZ, NY, NC, 32, DM), BF16),
            pltpu.VMEM((NZ, NY, NC, 32, DM), BF16),
            pltpu.VMEM((ROWS, DM), BF16),
            pltpu.VMEM((4, ROWS, OWN), BF16),
            pltpu.VMEM((6, ROWS // 2, OWN), BF16),
            dma((len(LOADS),)), dma((30,)), dma((30,)), dma((10,)), dma((10,)), dma((35,)), dma((35,)),
            dma((40,)), dma((40,)),
        ],
        compiler_params=pltpu.CompilerParams(
            collective_id=0, has_side_effects=True, vmem_limit_bytes=62 * 2**20
        ),
    )(*arrays)


def local(
    queries, keys, values, output_gate_logits, input_gate_log, forget_gate_logits, extra_decay_log,
    document, residual, cell_norm_gain, output_weight, mixer_norm_gain, up_weight, down_weight,
):
    return layer(
        input_gate_log.T, forget_gate_logits.T, extra_decay_log.T, document.reshape(1, ROWS),
        cell_norm_gain, mixer_norm_gain,
        queries, keys, values, output_gate_logits, residual, output_weight, up_weight, down_weight.T,
    )


def solution(mesh):
    split = Mesh(mesh.devices.reshape(NZ, NY, NC, NX), ("z", "y", "c", "x"))
    rows, heads = P(SP, "x"), P("x")
    return jax.shard_map(
        local,
        mesh=split,
        in_specs=(
            rows, rows, rows, rows, rows, rows, rows, P(SP), rows, heads, P("x", None), heads, rows, P("x", SP),
        ),
        out_specs=rows,
        check_vma=False,
    )
```

time: 172 us -> 92.6 us (0.54)
  waiting for transfers between devices: 43.8 us -> 0 us
  Pallas kernels: 54.5 us -> 90.6 us
  blocking collectives: 29.7 us -> 0 us
  matrix products: 15.9 us -> 0 us
  between operations: 13.4 us -> 0.01 us
  local copies, waits for them, and re-layouts: 9.24 us -> 1.87 us
  other arithmetic: 5.05 us -> 0 us
    all_gather x1 -> x0, waiting for transfers between devices: 43.8 us -> none  [local(): whole = lax.all_gather(both, SP, axis=0, tiled=True)]
    pallas_call x1, Pallas kernels: 54.5 us -> 90.6 us  [layer(): pl.pallas_call(kernel, out_shape=jax.ShapeDtypeStruct((ROWS, OWN), BF16),...]
    all_to_all x1 -> x0, blocking collectives: 29.7 us -> none  [summed_on_arrival(): lax.all_to_all(parts, axis, split_axis=0, concat_axis=0, tiled=True)]
    dot_general x1 -> x0, matrix products: 15.9 us -> none  [local(): lax.dot_general(squared, whole[:, DM:], (((1,), (1,)), ((), ())), preferr...]
    unnamed x12 -> x1, local copies, waits for them, and re-layouts: 6.06 us -> 1.87 us
    reshape x1 -> x0, local copies, waits for them, and re-layouts: 1.78 us -> none  [cut_along(): value.reshape(*lengths[:dim], count, lengths[dim] // count, *lengths[dim...]
  transfers between devices with their start and end apart: 1 -> 0, of which waited for: 1 -> 0; matrix products, arithmetic and copies ran while one was open for 2% -> 0% of each run, Pallas kernels for 32% -> 0%
where the time goes in v3:
time: 92.6 us; the launch traced here: 92.5 us
  Pallas kernels  90.6 us (98%)
  local copies, waits for them, and re-layouts  1.87 us (2%)
    pallas_call x1, Pallas kernels, layer(): pl.pallas_call(kernel, out_shape=jax.ShapeDtypeStruct((ROWS, OWN), BF16),...  90.6 us
    unnamed x1, local copies, waits for them, and re-layouts  1.87 us

profile of v3, /device:TPU:1, one launch (start us, length us, event | category | flops | bytes accessed | tf_op | source)
XLA Modules:
  0.0 92.5 jit_solution(10758936812935791870)
XLA Ops:
  0.0 90.6 %shard_map.136 = bf16[512,512]{1,0:T(8,128)(2,1)} custom-call(f32[2,512]{1,0:T(2,128)} %bitcast.6, f32[2,512]{1,0:T(2,128)} %bitcast.7, f32[2,512]{1,0:T(2,128)} %bitcast.8, s32[1,512]{1,0:T(1,128)} %bitcast.9, bf16[256]{0:T(256)(128)(2,1)} %cg_h.1, bf16[512]{0:T(512)(128)(2,1)} %mg_h.1, bf16[512,256]{1,0:T(8,128)(2,1)} %q_h.1, bf16[512,256]{1,0:T(8,128)(2,1)} %k_h.1, ...), custom_call_target="tpu_custom_call" | custom-call | tf_op jit(solution)/shard_map/pallas_call | solution.py:480
  90.6 1.9 %copy.16 = bf16[512,512]{1,0:T(8,128)(2,1)} copy(bf16[512,512]{1,0:T(8,128)(2,1)} %shard_map.136) | data formatting | bytes 1048576

commit v4 on v3

--- a/solution.py
+++ b/solution.py
@@ -20,20 +20,31 @@
 OFFS = (0, -1, 1, 2)
 LOADS = ("up", "down", "ig", "fg", "ex", "doc", "k", "v", "q", "cg", "og", "mg", "res", "w")
 
-RIGHT = (0, -1, 2)
+RIGHT = {"U": (0, -2, 2), "D": (0, -2, 2, -4)}
 
 ORDER = (
-    "begin", "gates", "state", "dz0,0", "wsend", "uz-1", "dy-1", "uz1", "dy1",
-    "st0", "y0", "uyz-1", "dz0,-1", "intra0", "uyz1", "do", "dz0,2", "st1",
-    "uz-2", "uz2", "uyz2", "intra1", "dz0,1", "cell", "dz-1,0", "ps1", "ufl",
-    "ufr", "uz-3", "uz3", "dz-1,2", "wpass", "uyz-3", "uyz3", "dz1,2", "dz-1,-1",
-    "dz1,1", "dz-1,1", "dm-1", "uyz-2", "dz1,-1", "outa", "dz1,0", "uz-4", "outb",
-    "ps-3", "dz-2,0", "dz2,-1", "dz2,2", "uyz-4", "dz-2,-1", "ps2", "ps3", "dz-2,1",
-    "ps-1", "ps0", "ps-2", "dm0", "ffr", "dz2,1", "dz-2,2", "dz2,0", "ps-4",
-    "ffl", "um0", "um-1", "um1", "dm2", "dz3,2", "dz3,1", "dm-2", "dz-3,0",
-    "dz-3,-1", "um2", "dz3,0", "dz3,-1", "norm", "up0", "dz4,1", "dz4,2", "dm3",
-    "dz-3,1", "dz-3,2", "dm1", "dm-3", "up1", "up2", "dz-4,0", "dz-4,-1", "dm4",
-    "up3", "down",
+    "tell", "begin", "Udy", "Uz0", "Dz0", "Ddy", "Uyz0", "Udz0,0", "intra0",
+    "wsend", "intra1", "Uz-1", "Uyz-1", "Uz1", "Dz-1", "Ddo", "Dz1", "Dyz-1",
+    "gsend", "st0", "Udz1,0", "Udz0,1", "Uz-2", "Udo", "Udz-1,0", "Uyz-2", "Uz2",
+    "Dyz0", "st1", "Dz-2", "Dz2", "Uyz2", "Udz0,-1", "Dyz-2", "comb", "cell0",
+    "Ups0", "Uyz1", "Uz-3", "cell1", "Udz1,1", "wpass", "Udz2,0", "Uz3", "Uyz3",
+    "Udz-1,1", "Uyz-3", "Udz0,2", "Dz3", "Dz-3", "Udm0", "Udz-1,-1", "Udz1,-1", "Dyz2",
+    "Udz-2,0", "ur0", "ul0", "Uz-4", "Uyz-4", "Um0", "Dyz1", "Udz2,1", "Dyz-3",
+    "Dyz3", "Udz3,0", "Ups2", "Dps-1", "Ups3", "Udz1,2", "Ups-3", "Udz-1,2", "Udz-2,1",
+    "ur1", "Ddz0,1", "Ups-1", "Ups1", "ul1", "Ups-2", "Udm-1", "Udm1", "Dps-2",
+    "out0", "Ddz0,0", "Ups-4", "Udz2,-1", "Udz-2,-1", "Dz-4", "Dm0", "Ddz0,-1", "Udz2,2",
+    "Ddz0,2", "Udm2", "Dyz-4", "Udz-3,0", "Udz3,1", "Um1", "Dps0", "Ddm0", "Dps1",
+    "Ddz1,1", "Udz-2,2", "Dps-3", "out1", "Dps2", "Um-1", "Udm-2", "Udz-3,1", "Udz3,-1",
+    "Dps3", "Ddz1,0", "Udz-3,-1", "Ddz-1,0", "fl0", "Udz3,2", "Ddz-1,-1", "Ddz1,2", "Ddz1,-1",
+    "fr0", "Ddm1", "Udm3", "Ddz-1,2", "Ddz2,1", "Ddz-1,1", "fl1", "Ddm-1", "Udz4,1",
+    "Udz-4,0", "Um2", "fr1", "Udz-3,2", "Udm-3", "Ddz2,0", "Udz-4,-1", "Udz4,2", "Udm4",
+    "Dps-4", "Dm-1", "norm0", "Ddz-2,0", "Ddz2,2", "up0,0", "Dm1", "Ddz-2,-1", "Ddz2,-1",
+    "up0,1", "Ddm2", "up0,2", "Ddz-2,2", "Ddz3,1", "norm1", "Dm2", "up0,3", "up1,0",
+    "Ddz-2,1", "Ddm-2", "up1,1", "s0,0", "Ddz3,2", "up1,2", "Ddz-3,0", "s0,1", "up1,3",
+    "Ddz-3,-1", "s1,0", "Ddz-3,2", "Ddz3,-1", "Ddz3,0", "Ddm3", "Ddz-3,1", "Ddm-3", "Ddz4,1",
+    "s1,1", "Ddz4,2", "j0,0", "s0,2", "Ddz-4,-1", "Ddz-4,0", "Ddm4", "s1,2", "s0,3",
+    "s1,3", "j1,1", "j0,1", "j1,0", "j0,2", "j1,2", "j0,3", "j1,3", "fin0",
+    "fin1",
 )
 
 
@@ -52,8 +63,8 @@
     ig_h, fg_h, ex_h, doc_h, cg_h, mg_h, q_h, k_h, v_h, og_h, res_h, wout_h, up_h, down_h,
     out,
     ig, fg, ex, doc, cg, mg, q, k, v, og, res, wc, nd, top, stin, auxin,
-    u, line1, line1in, full, line2, line2in, normed, wup, wdn, squared, terms, parts,
-    lsem, xss, xrs, sts, strs, uss, urs, dss, drs,
+    u, line1, line1in, full, line2, line2in, gains, normed, wup, wdn, squared, terms, parts,
+    lsem, xss, xrs, sts, strs, uss, urs, dss, drs, pss, prs,
 ):
     z, y, c, x = (lax.axis_index(a) for a in ("z", "y", "c", "x"))
     chip = z * NY + y
@@ -67,7 +78,7 @@
     zi = lambda o: lax.rem(z + NZ + o, NZ)
     xr, xl, yr, yl, zr, zl = ({a: f(o)} for a, f in (("x", xi), ("y", yi), ("z", zi)) for o in (1, -1))
     mate = {"c": 1 - c}
-    ahead, behind = at_chip(chip + 1), at_chip(chip - 1)
+    ahead, behind, two_ahead, two_behind = (at_chip(chip + o) for o in (1, -1, 2, -2))
     sp = chip * NC + c
 
     own_cols = pl.ds(pl.multiple_of(x * OWN, OWN), OWN)
@@ -82,11 +93,9 @@
         loads[name].start()
 
     barrier = pltpu.get_barrier_semaphore()
-    peers = [xr, xl, {"x": xi(2)}, mate, yr, yl, zr, zl, ahead, behind]
+    peers = [xr, xl, {"x": xi(2)}, mate, yr, yl, zr, zl, ahead, behind, two_ahead, two_behind]
     for peer in peers:
         pl.semaphore_signal(barrier, inc=1, device_id=peer, device_id_type=MESH)
-    pl.semaphore_wait(barrier, len(peers))
-
     pools = {"x": [xss, xrs, 0], "s": [sts, strs, 0], "u": [uss, urs, 0], "d": [dss, drs, 0]}
     copies = {}
 
@@ -111,84 +120,93 @@
         steps[f.__name__] = f
         return f
 
-    def up_at(zo, yo):
-        return wup.at[zi(zo), yi(yo), c]
-
-    def down_at(zo, yo):
-        return wdn.at[zi(zo), yi(yo), c]
-
     @step
     def begin():
         loads["up"].wait()
         loads["down"].wait()
-        own, dn = up_at(0, 0), down_at(0, 0)
-        send("u", "uz-1", own, own, zr)
-        send("u", "uz1", own, own, zl)
-        send("d", "dy-1", dn, dn, yr)
-        send("d", "dy1", dn, dn, yl)
-
-    def uz(zo):
-        arrived("uz%d" % zo)
-        ref = up_at(zo, 0)
-        if -4 < zo < 0:
-            send("u", "uz%d" % (zo - 1), ref, ref, zr)
-        elif 0 < zo < 3:
-            send("u", "uz%d" % (zo + 1), ref, ref, zl)
-
-    def uyz(zo):
-        ref = up_at(zo, 0)
-        send("u", "uy%d,-1" % zo, ref, ref, yr)
-        send("u", "uy%d,1" % zo, ref, ref, yl)
-
-    def ps(zo):
-        side = -1 if zo in RIGHT else 1
-        arrived("uy%d,%d" % (zo, side))
-        ref = up_at(zo, side)
-        send("u", "uo%d" % zo, ref, ref, yr if side < 0 else yl)
-
-    def um(yo):
-        if yo in (-1, 1):
-            arrived(*("uy%d,%d" % (zo, yo) for zo in range(-4, 4) if (zo in RIGHT) != (yo == -1)))
-        elif yo == 2:
-            arrived(*("uo%d" % zo for zo in range(-4, 4)))
-        ref = wup.at[:, yi(yo), c]
-        send("u", "umr%d" % yo, ref, ref, mate)
-
-    def dy(side):
-        arrived("dy%d" % side)
-        ref = wdn.at[z, yi(side), c, pl.ds(0 if side < 0 else 16, 16)]
-        send("d", "do%d" % side, ref, ref, yr if side < 0 else yl)
-
-    @step
-    def do():
-        arrived("do-1", "do1")
-
-    def dz(zo, yo):
-        ref = down_at(zo, yo)
-        if zo:
-            arrived("dz%d,%d" % (zo, yo))
-        for side, dev, last in ((-1, zr, (0, -1)), (1, zl, (1, 2))):
-            if zo * side < 0 or abs(zo) == 4 or (abs(zo) == 3 and yo not in last):
-                continue
-            send("d", "dz%d,%d" % (zo + side, yo), ref, ref, dev)
-
-    def dm(zo):
-        ref = wdn.at[zi(zo), :, c]
-        send("d", "dmr%d" % zo, ref, ref, mate)
-
-    for zo in range(-4, 4):
-        steps["uz%d" % zo] = lambda zo=zo: uz(zo)
-        steps["uyz%d" % zo] = lambda zo=zo: uyz(zo)
-        steps["ps%d" % zo] = lambda zo=zo: ps(zo)
-    steps["y0"] = steps["uyz0"]
-    for o in OFFS:
-        steps["um%d" % o] = lambda o=o: um(o)
-    for side in (-1, 1):
-        steps["dy%d" % side] = lambda side=side: dy(side)
-    for zo in range(-4, 5):
-        steps["dm%d" % zo] = lambda zo=zo: dm(zo)
-        for yo in OFFS:
-            steps["dz%d,%d" % (zo, yo)] = lambda zo=zo, yo=yo: dz(zo, yo)
+
+    def weight(w, pool, buf):
+        lo, hi = pl.ds(0, 16), pl.ds(16, 16)
+        at_lo = lambda zo, yo: buf.at[zi(zo), yi(yo), c, lo]
+        at_hi = lambda zo, yo: buf.at[zi(zo), yi(yo), c, hi]
+
+        def put(name, ref, dev):
+            send(pool, w + name, ref, ref, dev)
+
+        def come(*names):
+            arrived(*(w + name for name in names))
+
+        def along_z(zo):
+            if zo:
+                come("z%d" % zo)
+            if -4 < zo <= 0:
+                put("z%d" % (zo - 1), at_lo(zo, 0), zr)
+            if 0 <= zo < 3:
+                put("z%d" % (zo + 1), at_lo(zo, 0), zl)
+
+        def along_y(zo):
+            put("y%d,-1" % zo, at_lo(zo, 0), yr)
+            put("y%d,1" % zo, at_lo(zo, 0), yl)
+
+        def opposite(zo):
+            side = -1 if zo in RIGHT[w] else 1
+            come("y%d,%d" % (zo, side))
+            put("o%d" % zo, at_lo(zo, side), yr if side < 0 else yl)
+
+        def hand_y(yo):
+            if yo in (-1, 1):
+                come(*("y%d,%d" % (zo, yo) for zo in range(-4, 4) if (zo in RIGHT[w]) != (yo == -1)))
+            elif yo == 2:
+                come(*("o%d" % zo for zo in range(-4, 4)))
+            put("mr%d" % yo, buf.at[:, yi(yo), c, lo], mate)
+
+        def first_y():
+            put("dy-1", at_hi(0, 0), yr)
+            put("dy1", at_hi(0, 0), yl)
+
+        over = -1 if w == "U" else 1
+
+        def second_y():
+            come("dy%d" % over)
+            put("do", at_hi(0, over), yr if over < 0 else yl)
+
+        def then_z(zo, yo):
+            if zo:
+                come("dz%d,%d" % (zo, yo))
+            elif yo == -over:
+                come("dy%d" % yo)
+            elif yo == 2:
+                come("do")
+            for side, dev, last in ((-1, zr, (0, -1)), (1, zl, (1, 2))):
+                if zo * side < 0 or abs(zo) == 4 or (abs(zo) == 3 and yo not in last):
+                    continue
+                put("dz%d,%d" % (zo + side, yo), at_hi(zo, yo), dev)
+
+        def hand_z(zo):
+            put("dmr%d" % zo, buf.at[zi(zo), :, c, hi], mate)
+
+        for zo in range(-4, 4):
+            steps[w + "z%d" % zo] = lambda zo=zo: along_z(zo)
+            steps[w + "yz%d" % zo] = lambda zo=zo: along_y(zo)
+            steps[w + "ps%d" % zo] = lambda zo=zo: opposite(zo)
+        for o in OFFS:
+            steps[w + "m%d" % o] = lambda o=o: hand_y(o)
+        steps[w + "dy"] = first_y
+        steps[w + "do"] = second_y
+        for zo in range(-4, 5):
+            steps[w + "dm%d" % zo] = lambda zo=zo: hand_z(zo)
+            for yo in OFFS:
+                steps[w + "dz%d,%d" % (zo, yo)] = lambda zo=zo, yo=yo: then_z(zo, yo)
+
+    weight("U", "u", wup)
+    weight("D", "d", wdn)
+
+    @step
+    def gsend():
+        loads["mg"].wait()
+        gains[0] = jnp.broadcast_to(mg[...].astype(F32).reshape(1, OWN), (8, OWN))
+        for r in range(1, NX):
+            send("x", "g%d" % r, gains.at[0], gains.at[r], {"x": xi(r)})
 
     half = pl.multiple_of(c * 128, 128)
     wrows = lambda o: wc.at[pl.ds(pl.multiple_of(xi(o) * HW + half, 128), 128), :]
@@ -265,7 +283,11 @@
         auxin[5, 2:4] = got["between"](0, NB)
         auxin[5, 6:7] = got["last"]
         auxin[5, 7:8] = got["last"]
+
+    @step
+    def tell():
         pass_state(5, 0, ahead)
+        pass_state(5, 1, two_ahead)
         pass_state(5, 4, mate)
 
     def pass_state(slot, to, dev):
@@ -275,7 +297,6 @@
     @step
     def st0():
         arrived("st0", "sx0")
-        pass_state(0, 1, ahead)
         pass_state(0, 2, mate)
 
     @step
@@ -284,7 +305,9 @@
         pass_state(1, 3, mate)
 
     def intra(h):
-        loads["q"].wait() if h == 0 else None
+        if loads["q"] is not None:
+            loads["q"].wait()
+            loads["q"] = None
         vx = jnp.concatenate([v[:, head(h)], jnp.ones((ROWS, DH), BF16)], axis=1)
         for a in range(NB):
             n = (a + 1) * BLK
@@ -311,12 +334,36 @@
     steps["intra1"] = lambda: intra(1)
 
     ucols = lambda o: pl.ds(pl.multiple_of(xi(o) * HW, HW), HW)
-    uview = lambda o, s: u.at[pl.ds(256 * s, 256), ucols(o)]
+    def uview(o, s, part=None):
+        rows = pl.ds(256 * s, 256) if part is None else pl.ds(256 * s + 128 * part, 128)
+        return u.at[rows, ucols(o)]
+
     fcols = lambda o: pl.ds(pl.multiple_of(xi(o) * OWN, OWN), OWN)
-    fview = lambda o, s: full.at[pl.ds(256 * s, 256), fcols(o)]
-
-    @step
-    def cell():
+
+    def fview(o, s, part=None):
+        rows = pl.ds(256 * s, 256) if part is None else pl.ds(256 * s + 128 * part, 128)
+        return full.at[rows, fcols(o)]
+
+    def spread(view, tag, s):
+        send("x", tag + "%d-" % s, view(0, s), view(0, s), xr)
+        send("x", tag + "%d+" % s, view(0, s), view(0, s), xl)
+
+    def onward(view, tag, s, side):
+        if side < 0:
+            arrived(tag + "%d-" % s)
+            send("x", tag + "%dr" % s, view(-1, s, 0), view(-1, s, 0), xr)
+        else:
+            arrived(tag + "%d+" % s)
+            send("x", tag + "%dl" % s, view(1, s, 1), view(1, s, 1), xl)
+
+    for s in (0, 1):
+        steps["ur%d" % s] = lambda s=s: onward(uview, "u", s, -1)
+        steps["ul%d" % s] = lambda s=s: onward(uview, "u", s, 1)
+        steps["fr%d" % s] = lambda s=s: onward(fview, "f", s, -1)
+        steps["fl%d" % s] = lambda s=s: onward(fview, "f", s, 1)
+
+    @step
+    def comb():
         arrived("st2", "sx2", "st3", "sx3", "st4", "sx4")
         gone = jnp.zeros((2, BLK), F32)
         logs, slots = [], (2 + 2 * c, 0, 3 - c, 1)
@@ -335,8 +382,11 @@
             memx.append(jnp.concatenate([m, across(n)], axis=1).astype(BF16))
         loads["og"].wait()
         loads["cg"].wait()
-        gain = cg[...].astype(F32).reshape(1, HW)
-        for a in range(NB):
+        got.update(memx=memx, came=came, gain=cg[...].astype(F32).reshape(1, HW))
+
+    def cell(s):
+        memx, came, gain = got["memx"], got["came"], got["gain"]
+        for a in (2 * s, 2 * s + 1):
             squares = jnp.zeros((BLK, DH), F32)
             outs = []
             for h in range(2):
@@ -353,26 +403,26 @@
                 outs.append((gate * val * gain[:, head(h)]).astype(BF16))
             u[block(a), ucols(0)] = jnp.concatenate(outs, axis=1)
             line1[:, block(a)] = rows_of(squares)
-        send("x", "ua-", uview(0, 0), uview(0, 0), xr)
-        send("x", "ub+", uview(0, 1), uview(0, 1), xl)
+        cols = slice(256 * s, 256 * s + 256)
+        spread(uview, "u", s)
         for r in range(1, NX):
-            send("x", "l%d" % r, line1, line1in.at[r - 1], {"x": xi(r)})
-        send("x", "ub-", uview(0, 1), uview(0, 1), xr)
-        send("x", "ua+", uview(0, 0), uview(0, 0), xl)
-
-    @step
-    def ufr():
-        arrived("ua-")
-        send("x", "uar", uview(-1, 0), uview(-1, 0), xr)
-
-    @step
-    def ufl():
-        arrived("ub+")
-        send("x", "ubl", uview(1, 1), uview(1, 1), xl)
-
-    def project_out(s):
+            send("x", "l%d,%d" % (s, r), line1.at[:, cols], line1in.at[r - 1, :, cols], {"x": xi(r)})
+
+    steps["cell0"] = lambda: cell(0)
+    steps["cell1"] = lambda: cell(1)
+
+    def head_out(s):
+        arrived(*("l%d,%d" % (s, r) for r in range(1, NX)))
+        cols = slice(256 * s, 256 * s + 256)
+        total = line1[:, cols] + line1in[0, :, cols] + line1in[1, :, cols] + line1in[2, :, cols]
+        inv = lax.rsqrt(total / (DH * 8) + EPS)
+        if s == 0:
+            loads["w"].wait()
+            loads["res"].wait()
+            arrived("wm1", "wm2", "wm3")
+        arrived("u%dr" % s, "u%dl" % s)
         for a in (2 * s, 2 * s + 1):
-            ic = across(got["inv1"][0:1, block(a)])
+            ic = across(inv[0:1, block(a - 2 * s)])
             acc = jnp.dot(u[block(a), :], wc[...], preferred_element_type=F32)
             squares = jnp.zeros((BLK, BLK), F32)
             outs = []
@@ -384,91 +434,115 @@
             full[block(a), fcols(0)] = jnp.concatenate(outs, axis=1)
             line2[:, block(a)] = rows_of(squares)
 
-    @step
-    def outa():
-        arrived("l1", "l2", "l3")
-        total = line1[...] + line1in[0] + line1in[1] + line1in[2]
-        got["inv1"] = lax.rsqrt(total / (DH * 8) + EPS)
-        loads["w"].wait()
-        loads["res"].wait()
-        arrived("wm1", "wm2", "wm3", "ub-", "ua+", "uar", "ubl")
-        project_out(0)
-        send("x", "fa-", fview(0, 0), fview(0, 0), xr)
-        send("x", "fa+", fview(0, 0), fview(0, 0), xl)
-
-    @step
-    def outb():
-        project_out(1)
-        loads["mg"].wait()
-        line2[1:2, :] = mg[...].astype(F32).reshape(1, OWN)
+        spread(fview, "f", s)
         for r in range(1, NX):
-            send("x", "m%d" % r, line2, line2in.at[r - 1], {"x": xi(r)})
-        send("x", "fb-", fview(0, 1), fview(0, 1), xr)
-        send("x", "fb+", fview(0, 1), fview(0, 1), xl)
-
-    @step
-    def ffr():
-        arrived("fa-")
-        send("x", "far", fview(-1, 0), fview(-1, 0), xr)
-
-    @step
-    def ffl():
-        arrived("fb+")
-        send("x", "fbl", fview(1, 1), fview(1, 1), xl)
-
-    @step
-    def norm():
-        arrived("m1", "m2", "m3")
-        total = line2[...] + line2in[0] + line2in[1] + line2in[2]
+            send("x", "m%d,%d" % (s, r), line2.at[:, cols], line2in.at[r - 1, :, cols], {"x": xi(r)})
+
+    steps["out0"] = lambda: head_out(0)
+    steps["out1"] = lambda: head_out(1)
+
+    def norm(s):
+        arrived(*("m%d,%d" % (s, r) for r in range(1, NX)))
+        cols = slice(256 * s, 256 * s + 256)
+        total = line2[:, cols] + line2in[0, :, cols] + line2in[1, :, cols] + line2in[2, :, cols]
         inv = lax.rsqrt(total / DM + EPS)
-        arrived("fb-", "fa+", "far", "fbl")
-        icol = [across(inv[0:1, block(a)]) for a in range(NB)]
-        for r in range(NX):
-            gain = line2[1:2, :] if r == 0 else line2in[r - 1, 1:2, :]
-            for a in range(NB):
+        if s == 0:
+            arrived("g1", "g2", "g3")
+        arrived("f%dr" % s, "f%dl" % s)
+        for a in (2 * s, 2 * s + 1):
+            ic = across(inv[0:1, block(a - 2 * s)])
+            for r in range(NX):
                 fw = full[block(a), fcols(-r)].astype(F32)
+                gain = gains[0, 0:1] if r == 0 else gains[r, 0:1]
                 normed[block(a), fcols(-r)] = jnp.concatenate(
-                    [(fw[:, block(b)] * icol[a] * gain[:, block(b)]).astype(BF16) for b in range(OWN // BLK)], axis=1
+                    [(fw[:, block(b)] * ic * gain[:, block(b)]).astype(BF16) for b in range(OWN // BLK)], axis=1
                 )
 
-    def up(t):
-        if t == 0:
-            arrived("umr0", "umr-1", "umr1", "umr2")
-        cols = slice(t * 512, (t + 1) * 512)
-        hid = jnp.dot(normed[...], wup[:, :, :, :, cols].reshape(DM, 512), preferred_element_type=F32)
+    steps["norm0"] = lambda: norm(0)
+    steps["norm1"] = lambda: norm(1)
+
+    def up(s, t):
+        if s == t == 0:
+            arrived(*("Umr%d" % o for o in OFFS), *("Udmr%d" % zo for zo in range(-3, 5)))
+        rows, cols = slice(256 * s, 256 * s + 256), slice(t * 512, (t + 1) * 512)
+        hid = jnp.dot(normed[rows, :], wup[:, :, :, :, cols].reshape(DM, 512), preferred_element_type=F32)
         hid = jnp.maximum(hid, 0.0)
-        squared[:, cols] = (hid * hid).astype(BF16)
+        squared[rows, cols] = (hid * hid).astype(BF16)
 
     for t in range(4):
-        steps["up%d" % t] = lambda t=t: up(t)
-
-    @step
-    def down():
-        arrived(*("dmr%d" % zo for zo in range(-3, 5)))
-
-        def project(r):
-            w = wdn[pl.ds(2 * xi(r), 2)].reshape(OWN, DM)
-            return lax.dot_general(squared[...], w, (((1,), (1,)), ((), ())), preferred_element_type=F32)
-
-        a, b = slice(0, 256), slice(256, 512)
-        terms[2] = project(2).astype(BF16)
-        send("x", "p0", terms.at[2, a], parts.at[0], xr)
-        send("x", "p1", terms.at[2, b], parts.at[1], xl)
-        terms[1] = project(1).astype(BF16)
-        send("x", "p2", terms.at[1, b], parts.at[2], xr)
-        terms[3] = project(3).astype(BF16)
-        send("x", "p3", terms.at[3, a], parts.at[3], xl)
-        arrived("p0")
-        terms[1, a] = (terms[1, a].astype(F32) + parts[0].astype(F32)).astype(BF16)
-        send("x", "p4", terms.at[1, a], parts.at[4], xr)
-        arrived("p1")
-        terms[3, b] = (terms[3, b].astype(F32) + parts[1].astype(F32)).astype(BF16)
-        send("x", "p5", terms.at[3, b], parts.at[5], xl)
-        mine = project(0) + full[:, fcols(0)].astype(F32)
-        arrived("p2", "p3", "p4", "p5")
-        out[a] = (mine[a] + parts[3].astype(F32) + parts[4].astype(F32)).astype(BF16)
-        out[b] = (mine[b] + parts[2].astype(F32) + parts[5].astype(F32)).astype(BF16)
-
+        steps["up0,%d" % t] = lambda t=t: up(0, t)
+        steps["up1,%d" % t] = lambda t=t: up(1, t)
+
+    zb = lax.rem(z, 2)
+    owner = [lax.rem(z // 2 + d + NX, NX) for d in (0, 2 * zb - 1, 1 - 2 * zb, 2)]
+    ahead_by = [lax.rem(o - x + NX, NX) for o in owner]
+    ways = ((0, xr), (1, xl), (1, xr), (0, xl), (0, xr), (1, xl))
+    quarter = lambda s, h: slice(256 * s + 128 * h, 256 * s + 128 * h + 128)
+
+    def part(s, i, k):
+        h, dev = ways[i]
+        return pltpu.make_async_remote_copy(
+            src_ref=terms.at[k, quarter(s, h)], dst_ref=parts.at[s, i], send_sem=pss.at[6 * s + i],
+            recv_sem=prs.at[6 * s + i], device_id=dev, device_id_type=MESH,
+        )
+
+    def stage(s, k):
+        if s == 0:
+            if k == 0:
+                arrived(*("Dmr%d" % o for o in OFFS))
+            arrived(*("Ddmr%d" % zo for zo in ((0, 1, -1), (2, -2), (3, -3), (4,))[k]))
+        w = wdn[pl.ds(2 * owner[k], 2)].reshape(OWN, DM)
+        rows = slice(256 * s, 256 * s + 256)
+        terms[k, rows] = lax.dot_general(
+            squared[rows, :], w, (((1,), (1,)), ((), ())), preferred_element_type=F32
+        ).astype(BF16)
+
+        @pl.when(ahead_by[k] == 2)
+        def _():
+            part(s, 0, k).start()
+            part(s, 1, k).start()
+
+        @pl.when(ahead_by[k] == 1)
+        def _():
+            part(s, 2, k).start()
+
+        @pl.when(ahead_by[k] == 3)
+        def _():
+            part(s, 3, k).start()
+
+    def join(s, k):
+        for side, h, i in ((1, 0, 0), (3, 1, 1)):
+            @pl.when(ahead_by[k] == side)
+            def _():
+                part(s, i, 0).wait_recv()
+                rows = quarter(s, h)
+                terms[k, rows] = (terms[k, rows].astype(F32) + parts[s, i].astype(F32)).astype(BF16)
+                part(s, i + 4, k).start()
+
+    def final(s):
+        d = lax.rem(x - z // 2 + NX, NX)
+        d = lax.rem(d * (2 * zb - 1) + NX, NX)
+        mine = terms.at[d + d // 2 - 2 * (d // 3)]
+        for h, i, n in ((0, 3, 4), (1, 2, 5)):
+            part(s, i, 0).wait_recv()
+            part(s, n, 0).wait_recv()
+            rows = quarter(s, h)
+            out[rows] = (
+                full[rows, fcols(0)].astype(F32) + mine[rows].astype(F32)
+                + parts[s, i].astype(F32) + parts[s, n].astype(F32)
+            ).astype(BF16)
+        for i in range(6):
+            part(s, i, 0).wait_send()
+
+    for s in (0, 1):
+        for n in range(4):
+            steps["s%d,%d" % (s, n)] = lambda s=s, n=n: stage(s, n)
+            steps["j%d,%d" % (s, n)] = lambda s=s, n=n: join(s, n)
+        steps["fin%d" % s] = lambda s=s: final(s)
+
+    steps["gates"]()
+    steps["state"]()
+    pl.semaphore_wait(barrier, len(peers))
     for name in ORDER:
         steps[name]()
     for d in copies.values():
@@ -495,14 +569,15 @@
             pltpu.VMEM((ROWS, DM), BF16),
             pltpu.VMEM((8, ROWS), F32),
             pltpu.VMEM((3, 8, ROWS), F32),
+            pltpu.VMEM((4, 8, OWN), F32),
             pltpu.VMEM((ROWS, DM), BF16),
             pltpu.VMEM((NZ, NY, NC, 32, DM), BF16),
             pltpu.VMEM((NZ, NY, NC, 32, DM), BF16),
             pltpu.VMEM((ROWS, DM), BF16),
             pltpu.VMEM((4, ROWS, OWN), BF16),
-            pltpu.VMEM((6, ROWS // 2, OWN), BF16),
-            dma((len(LOADS),)), dma((30,)), dma((30,)), dma((10,)), dma((10,)), dma((35,)), dma((35,)),
-            dma((40,)), dma((40,)),
+            pltpu.VMEM((2, 6, ROWS // 4, OWN), BF16),
+            dma((len(LOADS),)), dma((37,)), dma((37,)), dma((10,)), dma((10,)), dma((75,)), dma((75,)),
+            dma((75,)), dma((75,)), dma((12,)), dma((12,)),
         ],
         compiler_params=pltpu.CompilerParams(
             collective_id=0, has_side_effects=True, vmem_limit_bytes=62 * 2**20

time: 92.6 us -> 89.1 us (0.962)
  Pallas kernels: 90.6 us -> 86.8 us
    pallas_call x1, Pallas kernels: 90.6 us -> 86.8 us  [layer(): pl.pallas_call(kernel, out_shape=jax.ShapeDtypeStruct((ROWS, OWN), BF16),...]
where the time goes in v4:
time: 89.1 us; the launch traced here: 88.7 us
  Pallas kernels  86.8 us (97%)
  local copies, waits for them, and re-layouts  1.87 us (2%)
    pallas_call x1, Pallas kernels, layer(): pl.pallas_call(kernel, out_shape=jax.ShapeDtypeStruct((ROWS, OWN), BF16),...  86.8 us
    unnamed x1, local copies, waits for them, and re-layouts  1.87 us

profile of v4, /device:TPU:1, one launch (start us, length us, event | category | flops | bytes accessed | tf_op | source)
XLA Modules:
  0.0 88.7 jit_solution(1149488403722175775)
XLA Ops:
  0.0 86.8 %shard_map.136 = bf16[512,512]{1,0:T(8,128)(2,1)} custom-call(f32[2,512]{1,0:T(2,128)} %bitcast.6, f32[2,512]{1,0:T(2,128)} %bitcast.7, f32[2,512]{1,0:T(2,128)} %bitcast.8, s32[1,512]{1,0:T(1,128)} %bitcast.9, bf16[256]{0:T(256)(128)(2,1)} %cg_h.1, bf16[512]{0:T(512)(128)(2,1)} %mg_h.1, bf16[512,256]{1,0:T(8,128)(2,1)} %q_h.1, bf16[512,256]{1,0:T(8,128)(2,1)} %k_h.1, ...), custom_call_target="tpu_custom_call" | custom-call | tf_op jit(solution)/shard_map/pallas_call | solution.py:554
  86.8 1.9 %copy.16 = bf16[512,512]{1,0:T(8,128)(2,1)} copy(bf16[512,512]{1,0:T(8,128)(2,1)} %shard_map.136) | data formatting | bytes 1048576

commit v5 on v4

--- a/solution.py
+++ b/solution.py
@@ -20,31 +20,35 @@
 OFFS = (0, -1, 1, 2)
 LOADS = ("up", "down", "ig", "fg", "ex", "doc", "k", "v", "q", "cg", "og", "mg", "res", "w")
 
-RIGHT = {"U": (0, -2, 2), "D": (0, -2, 2, -4)}
+RIGHT = {"U": (0, -2, 2, -4), "D": (0, -2, 2)}
+SPLIT = {"U": 16, "D": 24}
+
+RECEIVES = 164
 
 ORDER = (
-    "tell", "begin", "Udy", "Uz0", "Dz0", "Ddy", "Uyz0", "Udz0,0", "intra0",
-    "wsend", "intra1", "Uz-1", "Uyz-1", "Uz1", "Dz-1", "Ddo", "Dz1", "Dyz-1",
-    "gsend", "st0", "Udz1,0", "Udz0,1", "Uz-2", "Udo", "Udz-1,0", "Uyz-2", "Uz2",
-    "Dyz0", "st1", "Dz-2", "Dz2", "Uyz2", "Udz0,-1", "Dyz-2", "comb", "cell0",
-    "Ups0", "Uyz1", "Uz-3", "cell1", "Udz1,1", "wpass", "Udz2,0", "Uz3", "Uyz3",
-    "Udz-1,1", "Uyz-3", "Udz0,2", "Dz3", "Dz-3", "Udm0", "Udz-1,-1", "Udz1,-1", "Dyz2",
-    "Udz-2,0", "ur0", "ul0", "Uz-4", "Uyz-4", "Um0", "Dyz1", "Udz2,1", "Dyz-3",
-    "Dyz3", "Udz3,0", "Ups2", "Dps-1", "Ups3", "Udz1,2", "Ups-3", "Udz-1,2", "Udz-2,1",
-    "ur1", "Ddz0,1", "Ups-1", "Ups1", "ul1", "Ups-2", "Udm-1", "Udm1", "Dps-2",
-    "out0", "Ddz0,0", "Ups-4", "Udz2,-1", "Udz-2,-1", "Dz-4", "Dm0", "Ddz0,-1", "Udz2,2",
-    "Ddz0,2", "Udm2", "Dyz-4", "Udz-3,0", "Udz3,1", "Um1", "Dps0", "Ddm0", "Dps1",
-    "Ddz1,1", "Udz-2,2", "Dps-3", "out1", "Dps2", "Um-1", "Udm-2", "Udz-3,1", "Udz3,-1",
-    "Dps3", "Ddz1,0", "Udz-3,-1", "Ddz-1,0", "fl0", "Udz3,2", "Ddz-1,-1", "Ddz1,2", "Ddz1,-1",
-    "fr0", "Ddm1", "Udm3", "Ddz-1,2", "Ddz2,1", "Ddz-1,1", "fl1", "Ddm-1", "Udz4,1",
-    "Udz-4,0", "Um2", "fr1", "Udz-3,2", "Udm-3", "Ddz2,0", "Udz-4,-1", "Udz4,2", "Udm4",
-    "Dps-4", "Dm-1", "norm0", "Ddz-2,0", "Ddz2,2", "up0,0", "Dm1", "Ddz-2,-1", "Ddz2,-1",
-    "up0,1", "Ddm2", "up0,2", "Ddz-2,2", "Ddz3,1", "norm1", "Dm2", "up0,3", "up1,0",
-    "Ddz-2,1", "Ddm-2", "up1,1", "s0,0", "Ddz3,2", "up1,2", "Ddz-3,0", "s0,1", "up1,3",
-    "Ddz-3,-1", "s1,0", "Ddz-3,2", "Ddz3,-1", "Ddz3,0", "Ddm3", "Ddz-3,1", "Ddm-3", "Ddz4,1",
-    "s1,1", "Ddz4,2", "j0,0", "s0,2", "Ddz-4,-1", "Ddz-4,0", "Ddm4", "s1,2", "s0,3",
-    "s1,3", "j1,1", "j0,1", "j1,0", "j0,2", "j1,2", "j0,3", "j1,3", "fin0",
-    "fin1",
+    "tell", "begin", "Uz0", "Ddz0,0", "wsend", "Udy", "Ddy", "Dz0", "gsend",
+    "intra0", "Dyz0", "Uz-1", "Uz1", "Uyz1", "Ddo", "Uyz-1", "Udz0,0", "st0",
+    "intra1", "Dz1", "Dz-1", "Uz-2", "Ups1", "Udo", "Uz2", "Udz0,1", "st1",
+    "Ddz0,1", "Udz1,0", "Dyz-1", "Uyz-2", "comb", "Ddz0,2", "cell0", "Dyz1", "Udz0,-1",
+    "Uz-3", "Udz-1,0", "Um1", "cell1", "Uz3", "wpass", "Udz0,2", "Udz-1,1", "Udm0",
+    "Udz1,1", "Ups-1", "Uyz3", "Dps-1", "Dz-2", "Udz-1,-1", "Ddz0,-1", "Uyz-3", "Ddm0",
+    "ul0", "Udz2,0", "Ddz1,0", "Ddz1,1", "ur0", "Uyz0", "Uyz2", "Uz-4", "Udz-2,0",
+    "Udz1,2", "ul1", "ur1", "Udz1,-1", "Udz-1,2", "Ddz1,2", "Udm-1", "Dps1", "out0",
+    "Ups3", "Udz3,0", "Uyz-4", "Ddz1,-1", "Udz2,1", "Dyz-2", "out1", "Udz-2,-1", "Ups2",
+    "Udz-2,1", "Dm-1", "Udz2,2", "Ups-3", "Ups0", "Udz2,-1", "Udz-3,0", "Dz2", "Udz-2,2",
+    "Dyz2", "Udz3,1", "Ups-4", "Udz3,2", "Ups-2", "Ddz2,1", "Udm-2", "Ddz2,-1", "Dps0",
+    "Ddz2,2", "fl0", "Dm1", "Udz-3,-1", "Dz-3", "Ddz-1,-1", "Ddz-1,0", "fr0", "Ddz2,0",
+    "Ddz-1,2", "Ddz-1,1", "Udm2", "Um0", "Udz3,-1", "Um-1", "Udm3", "Um3", "Udz-3,1",
+    "Ddm2", "Dps-2", "Udm1", "Um2", "Ddm1", "Dps2", "Dyz-3", "Um-3", "Um-4",
+    "Udz-3,2", "Ddm-1", "Udz-4,0", "Udz-4,-1", "Dz3", "Udm-3", "Dyz3", "fl1", "Udz4,1",
+    "Um-2", "Udz4,2", "Udm4", "Ddz3,1", "fr1", "Dz-4", "Dyz-4", "Ddz3,-1", "Dps-3",
+    "norm0", "Ddz-2,0", "up0,0", "Ddz-2,2", "Ddz-2,-1", "Dm0", "Ddz3,0", "up0,1", "Ddz3,2",
+    "Ddm3", "Dps3", "Ddz-2,1", "up0,2", "Ddm-2", "Dm-2", "up0,3", "Ddz4,1", "s0,0",
+    "Dm2", "Ddz-3,0", "Dps-4", "norm1", "up1,0", "up1,1", "Ddz4,2", "Ddz-3,-1", "Ddz-3,2",
+    "s0,1", "Dm-3", "Ddz-3,1", "up1,2", "Ddm-3", "up1,3", "Ddz-4,0", "Dm3", "s1,0",
+    "Ddz-4,-1", "Ddm4", "Dm-4", "s1,1", "s0,2", "j0,1", "s1,2", "s0,3", "j0,0",
+    "s1,3", "j1,0", "j0,2", "j1,2", "j1,1", "j0,3", "j1,3", "sent", "fin0",
+    "fin1", "rest",
 )
 
 
@@ -61,10 +65,10 @@
 
 def kernel(
     ig_h, fg_h, ex_h, doc_h, cg_h, mg_h, q_h, k_h, v_h, og_h, res_h, wout_h, up_h, down_h,
-    out,
+    out_h,
     ig, fg, ex, doc, cg, mg, q, k, v, og, res, wc, nd, top, stin, auxin,
-    u, line1, line1in, full, line2, line2in, gains, normed, wup, wdn, squared, terms, parts,
-    lsem, xss, xrs, sts, strs, uss, urs, dss, drs, pss, prs,
+    u, line1, line1in, full, line2, line2in, gains, normed, wup, wdn, squared, terms, parts, out,
+    lsem, ssem, rsem, prs, osem,
 ):
     z, y, c, x = (lax.axis_index(a) for a in ("z", "y", "c", "x"))
     chip = z * NY + y
@@ -96,16 +100,28 @@
     peers = [xr, xl, {"x": xi(2)}, mate, yr, yl, zr, zl, ahead, behind, two_ahead, two_behind]
     for peer in peers:
         pl.semaphore_signal(barrier, inc=1, device_id=peer, device_id_type=MESH)
-    pools = {"x": [xss, xrs, 0], "s": [sts, strs, 0], "u": [uss, urs, 0], "d": [dss, drs, 0]}
-    copies = {}
-
-    def send(pool, name, src, dst, dev):
-        p = pools[pool]
+    copies, shared = {}, {}
+    sizes = {
+        "U1": wup.at[0:7, 0, 0], "U2": wup.at[0:7], "D1": wdn.at[0:7, 0, 0], "D2": wdn.at[0:7],
+        "u": u.at[0:384], "f": full.at[0:384], "l": line1in, "m": line2in, "g": gains.at[0:3],
+        "w": wc.at[0:384], "wm": wc.at[0:384], "st": stin.at[0:5], "sx": auxin.at[0:5], "p": parts,
+    }
+    groups = list(sizes)
+    counts = [0]
+
+    def receive(key=None):
+        if key in shared:
+            return shared[key]
+        counts[0] += 1
+        if key is not None:
+            shared[key] = counts[0] - 1
+        return counts[0] - 1
+
+    def send(group, name, src, dst, dev, key=None):
         d = pltpu.make_async_remote_copy(
-            src_ref=src, dst_ref=dst, send_sem=p[0].at[p[2]], recv_sem=p[1].at[p[2]],
+            src_ref=src, dst_ref=dst, send_sem=ssem.at[groups.index(group)], recv_sem=rsem.at[receive(key)],
             device_id=dev, device_id_type=MESH,
         )
-        p[2] += 1
         d.start()
         copies[name] = d
 
@@ -113,6 +129,12 @@
         for name in names:
             copies[name].wait_recv()
 
+    def all_arrived(key, ref):
+        pltpu.make_async_copy(ref, ref, rsem.at[shared[key]]).wait()
+
+    def all_sent(group):
+        pltpu.make_async_copy(sizes[group], sizes[group], ssem.at[groups.index(group)]).wait()
+
     got = {}
     steps = {}
 
@@ -125,16 +147,20 @@
         loads["up"].wait()
         loads["down"].wait()
 
-    def weight(w, pool, buf):
-        lo, hi = pl.ds(0, 16), pl.ds(16, 16)
+    def weight(w, buf):
+        lo, hi = pl.ds(0, SPLIT[w]), pl.ds(SPLIT[w], 32 - SPLIT[w])
         at_lo = lambda zo, yo: buf.at[zi(zo), yi(yo), c, lo]
         at_hi = lambda zo, yo: buf.at[zi(zo), yi(yo), c, hi]
 
-        def put(name, ref, dev):
-            send(pool, w + name, ref, ref, dev)
+        early = ["dz%d,%d" % (zo, yo) for zo in (-1, 1, -2, 2, -3, 3, -4, 4) for yo in OFFS][:14 if w == "U" else 32]
+
+        def put(name, ref, dev, key=None):
+            send(w + ("1" if name in early else "2"), w + name, ref, ref, dev, key)
 
         def come(*names):
             arrived(*(w + name for name in names))
+
+        mates = lambda zo: "U" if w == "U" else "D%d" % max(abs(zo) - 1, 0)
 
         def along_z(zo):
             if zo:
@@ -153,12 +179,9 @@
             come("y%d,%d" % (zo, side))
             put("o%d" % zo, at_lo(zo, side), yr if side < 0 else yl)
 
-        def hand_y(yo):
-            if yo in (-1, 1):
-                come(*("y%d,%d" % (zo, yo) for zo in range(-4, 4) if (zo in RIGHT[w]) != (yo == -1)))
-            elif yo == 2:
-                come(*("o%d" % zo for zo in range(-4, 4)))
-            put("mr%d" % yo, buf.at[:, yi(yo), c, lo], mate)
+        def hand_y(zo):
+            come("y%d,%d" % (zo, 1 if zo in RIGHT[w] else -1), "o%d" % zo)
+            put("mr%d" % zo, buf.at[zi(zo), :, c, lo], mate, mates(zo))
 
         def first_y():
             put("dy-1", at_hi(0, 0), yr)
@@ -183,14 +206,13 @@
                 put("dz%d,%d" % (zo + side, yo), at_hi(zo, yo), dev)
 
         def hand_z(zo):
-            put("dmr%d" % zo, buf.at[zi(zo), :, c, hi], mate)
+            put("dmr%d" % zo, buf.at[zi(zo), :, c, hi], mate, mates(zo))
 
         for zo in range(-4, 4):
             steps[w + "z%d" % zo] = lambda zo=zo: along_z(zo)
             steps[w + "yz%d" % zo] = lambda zo=zo: along_y(zo)
             steps[w + "ps%d" % zo] = lambda zo=zo: opposite(zo)
-        for o in OFFS:
-            steps[w + "m%d" % o] = lambda o=o: hand_y(o)
+            steps[w + "m%d" % zo] = lambda zo=zo: hand_y(zo)
         steps[w + "dy"] = first_y
         steps[w + "do"] = second_y
         for zo in range(-4, 5):
@@ -198,15 +220,15 @@
             for yo in OFFS:
                 steps[w + "dz%d,%d" % (zo, yo)] = lambda zo=zo, yo=yo: then_z(zo, yo)
 
-    weight("U", "u", wup)
-    weight("D", "d", wdn)
+    weight("U", wup)
+    weight("D", wdn)
 
     @step
     def gsend():
         loads["mg"].wait()
         gains[0] = jnp.broadcast_to(mg[...].astype(F32).reshape(1, OWN), (8, OWN))
         for r in range(1, NX):
-            send("x", "g%d" % r, gains.at[0], gains.at[r], {"x": xi(r)})
+            send("g", "g%d" % r, gains.at[0], gains.at[r], {"x": xi(r)}, "g")
 
     half = pl.multiple_of(c * 128, 128)
     wrows = lambda o: wc.at[pl.ds(pl.multiple_of(xi(o) * HW + half, 128), 128), :]
@@ -215,13 +237,13 @@
     def wsend():
         for r in range(1, NX):
             cols = pl.ds(pl.multiple_of(xi(r) * OWN, OWN), OWN)
-            send("x", "w%d" % r, wout_h.at[pl.ds(half, 128), cols], wrows(0), {"x": xi(r)})
+            send("w", "w%d" % r, wout_h.at[pl.ds(half, 128), cols], wrows(0), {"x": xi(r)})
 
     @step
     def wpass():
         for r in range(1, NX):
             arrived("w%d" % r)
-            send("x", "wm%d" % r, wrows(-r), wrows(-r), mate)
+            send("wm", "wm%d" % r, wrows(-r), wrows(-r), mate, "wm")
 
     ri = lax.broadcasted_iota(jnp.int32, (BLK, BLK), 0)
     ci = lax.broadcasted_iota(jnp.int32, (BLK, BLK), 1)
@@ -291,8 +313,8 @@
         pass_state(5, 4, mate)
 
     def pass_state(slot, to, dev):
-        send("s", "st%d" % to, stin.at[slot], stin.at[to], dev)
-        send("s", "sx%d" % to, auxin.at[slot], auxin.at[to], dev)
+        send("st", "st%d" % to, stin.at[slot], stin.at[to], dev)
+        send("sx", "sx%d" % to, auxin.at[slot], auxin.at[to], dev)
 
     @step
     def st0():
@@ -345,16 +367,16 @@
         return full.at[rows, fcols(o)]
 
     def spread(view, tag, s):
-        send("x", tag + "%d-" % s, view(0, s), view(0, s), xr)
-        send("x", tag + "%d+" % s, view(0, s), view(0, s), xl)
+        send(tag, tag + "%d-" % s, view(0, s), view(0, s), xr)
+        send(tag, tag + "%d+" % s, view(0, s), view(0, s), xl)
 
     def onward(view, tag, s, side):
         if side < 0:
             arrived(tag + "%d-" % s)
-            send("x", tag + "%dr" % s, view(-1, s, 0), view(-1, s, 0), xr)
+            send(tag, tag + "%dr" % s, view(-1, s, 0), view(-1, s, 0), xr)
         else:
             arrived(tag + "%d+" % s)
-            send("x", tag + "%dl" % s, view(1, s, 1), view(1, s, 1), xl)
+            send(tag, tag + "%dl" % s, view(1, s, 1), view(1, s, 1), xl)
 
     for s in (0, 1):
         steps["ur%d" % s] = lambda s=s: onward(uview, "u", s, -1)
@@ -406,20 +428,20 @@
         cols = slice(256 * s, 256 * s + 256)
         spread(uview, "u", s)
         for r in range(1, NX):
-            send("x", "l%d,%d" % (s, r), line1.at[:, cols], line1in.at[r - 1, :, cols], {"x": xi(r)})
+            send("l", "l%d,%d" % (s, r), line1.at[:, cols], line1in.at[r - 1, :, cols], {"x": xi(r)}, "l%d" % s)
 
     steps["cell0"] = lambda: cell(0)
     steps["cell1"] = lambda: cell(1)
 
     def head_out(s):
-        arrived(*("l%d,%d" % (s, r) for r in range(1, NX)))
         cols = slice(256 * s, 256 * s + 256)
+        all_arrived("l%d" % s, line1in.at[:, :, cols])
         total = line1[:, cols] + line1in[0, :, cols] + line1in[1, :, cols] + line1in[2, :, cols]
         inv = lax.rsqrt(total / (DH * 8) + EPS)
         if s == 0:
             loads["w"].wait()
             loads["res"].wait()
-            arrived("wm1", "wm2", "wm3")
+            all_arrived("wm", wc.at[0:384])
         arrived("u%dr" % s, "u%dl" % s)
         for a in (2 * s, 2 * s + 1):
             ic = across(inv[0:1, block(a - 2 * s)])
@@ -436,18 +458,18 @@
 
         spread(fview, "f", s)
         for r in range(1, NX):
-            send("x", "m%d,%d" % (s, r), line2.at[:, cols], line2in.at[r - 1, :, cols], {"x": xi(r)})
+            send("m", "m%d,%d" % (s, r), line2.at[:, cols], line2in.at[r - 1, :, cols], {"x": xi(r)}, "m%d" % s)
 
     steps["out0"] = lambda: head_out(0)
     steps["out1"] = lambda: head_out(1)
 
     def norm(s):
-        arrived(*("m%d,%d" % (s, r) for r in range(1, NX)))
         cols = slice(256 * s, 256 * s + 256)
+        all_arrived("m%d" % s, line2in.at[:, :, cols])
         total = line2[:, cols] + line2in[0, :, cols] + line2in[1, :, cols] + line2in[2, :, cols]
         inv = lax.rsqrt(total / DM + EPS)
         if s == 0:
-            arrived("g1", "g2", "g3")
+            all_arrived("g", gains.at[0:3])
         arrived("f%dr" % s, "f%dl" % s)
         for a in (2 * s, 2 * s + 1):
             ic = across(inv[0:1, block(a - 2 * s)])
@@ -463,7 +485,7 @@
 
     def up(s, t):
         if s == t == 0:
-            arrived(*("Umr%d" % o for o in OFFS), *("Udmr%d" % zo for zo in range(-3, 5)))
+            all_arrived("U", wup.at[0:4])
         rows, cols = slice(256 * s, 256 * s + 256), slice(t * 512, (t + 1) * 512)
         hid = jnp.dot(normed[rows, :], wup[:, :, :, :, cols].reshape(DM, 512), preferred_element_type=F32)
         hid = jnp.maximum(hid, 0.0)
@@ -482,15 +504,13 @@
     def part(s, i, k):
         h, dev = ways[i]
         return pltpu.make_async_remote_copy(
-            src_ref=terms.at[k, quarter(s, h)], dst_ref=parts.at[s, i], send_sem=pss.at[6 * s + i],
+            src_ref=terms.at[k, quarter(s, h)], dst_ref=parts.at[s, i], send_sem=ssem.at[groups.index("p")],
             recv_sem=prs.at[6 * s + i], device_id=dev, device_id_type=MESH,
         )
 
     def stage(s, k):
         if s == 0:
-            if k == 0:
-                arrived(*("Dmr%d" % o for o in OFFS))
-            arrived(*("Ddmr%d" % zo for zo in ((0, 1, -1), (2, -2), (3, -3), (4,))[k]))
+            all_arrived("D%d" % k, (wdn.at[0:3, :, 0], wdn.at[0], wdn.at[0], wdn.at[0, :, 0])[k])
         w = wdn[pl.ds(2 * owner[k], 2)].reshape(OWN, DM)
         rows = slice(256 * s, 256 * s + 256)
         terms[k, rows] = lax.dot_general(
@@ -518,6 +538,12 @@
                 rows = quarter(s, h)
                 terms[k, rows] = (terms[k, rows].astype(F32) + parts[s, i].astype(F32)).astype(BF16)
                 part(s, i + 4, k).start()
+
+    @step
+    def sent():
+        for group in groups:
+            if group != "p":
+                all_sent(group)
 
     def final(s):
         d = lax.rem(x - z // 2 + NX, NX)
@@ -531,8 +557,18 @@
                 full[rows, fcols(0)].astype(F32) + mine[rows].astype(F32)
                 + parts[s, i].astype(F32) + parts[s, n].astype(F32)
             ).astype(BF16)
-        for i in range(6):
-            part(s, i, 0).wait_send()
+        half = slice(256 * s, 256 * s + 256)
+        d = pltpu.make_async_copy(out.at[half], out_h.at[half], osem.at[s])
+        d.start()
+        kept.append(d)
+
+    kept = []
+
+    @step
+    def rest():
+        for d in kept:
+            d.wait()
+        all_sent("p")
 
     for s in (0, 1):
         for n in range(4):
@@ -545,8 +581,6 @@
     pl.semaphore_wait(barrier, len(peers))
     for name in ORDER:
         steps[name]()
-    for d in copies.values():
-        d.wait_send()
 
 
 def layer(*arrays):
@@ -555,7 +589,7 @@
         kernel,
         out_shape=jax.ShapeDtypeStruct((ROWS, OWN), BF16),
         in_specs=[pl.BlockSpec(memory_space=pltpu.HBM)] * len(arrays),
-        out_specs=pl.BlockSpec(memory_space=pltpu.VMEM),
+        out_specs=pl.BlockSpec(memory_space=pltpu.HBM),
         scratch_shapes=[
             *[pltpu.VMEM(a.shape, a.dtype) for a in arrays[:11]],
             pltpu.VMEM((4 * HW, OWN), BF16),
@@ -576,8 +610,8 @@
             pltpu.VMEM((ROWS, DM), BF16),
             pltpu.VMEM((4, ROWS, OWN), BF16),
             pltpu.VMEM((2, 6, ROWS // 4, OWN), BF16),
-            dma((len(LOADS),)), dma((37,)), dma((37,)), dma((10,)), dma((10,)), dma((75,)), dma((75,)),
-            dma((75,)), dma((75,)), dma((12,)), dma((12,)),
+            pltpu.VMEM((ROWS, OWN), BF16),
+            dma((len(LOADS),)), dma((14,)), dma((RECEIVES,)), dma((12,)), dma((2,)),
         ],
         compiler_params=pltpu.CompilerParams(
             collective_id=0, has_side_effects=True, vmem_limit_bytes=62 * 2**20

time: 89.1 us -> 86 us (0.965); the launches traced: 88.7 us -> 84.6 us
  Pallas kernels: 86.8 us -> 82.7 us
    pallas_call x1, Pallas kernels: 86.8 us -> 82.7 us  [layer(): pl.pallas_call(kernel, out_shape=jax.ShapeDtypeStruct((ROWS, OWN), BF16),...]
where the time goes in v5:
time: 86 us; the launch traced here: 84.6 us
  Pallas kernels  82.7 us (96%)
  local copies, waits for them, and re-layouts  1.87 us (2%)
    pallas_call x1, Pallas kernels, layer(): pl.pallas_call(kernel, out_shape=jax.ShapeDtypeStruct((ROWS, OWN), BF16),...  82.7 us
    unnamed x1, local copies, waits for them, and re-layouts  1.87 us

profile of v5, /device:TPU:1, one launch (start us, length us, event | category | flops | bytes accessed | tf_op | source)
XLA Modules:
  0.0 84.6 jit_solution(17579386462959249515)
XLA Ops:
  0.0 82.7 %shard_map.136 = bf16[512,512]{1,0:T(8,128)(2,1)} custom-call(f32[2,512]{1,0:T(2,128)} %bitcast.6, f32[2,512]{1,0:T(2,128)} %bitcast.7, f32[2,512]{1,0:T(2,128)} %bitcast.8, s32[1,512]{1,0:T(1,128)} %bitcast.9, bf16[256]{0:T(256)(128)(2,1)} %cg_h.1, bf16[512]{0:T(512)(128)(2,1)} %mg_h.1, bf16[512,256]{1,0:T(8,128)(2,1)} %q_h.1, bf16[512,256]{1,0:T(8,128)(2,1)} %k_h.1, ...), custom_call_target="tpu_custom_call" | custom-call | tf_op jit(solution)/shard_map/pallas_call | solution.py:588
  82.7 1.9 %copy.16 = bf16[512,512]{1,0:T(8,128)(2,1)} copy(bf16[512,512]{1,0:T(8,128)(2,1)} %shard_map.136) | data formatting | bytes 1048576

commit v6 on v5

--- a/solution.py
+++ b/solution.py
@@ -26,27 +26,27 @@
 RECEIVES = 164
 
 ORDER = (
-    "tell", "begin", "Uz0", "Ddz0,0", "wsend", "Udy", "Ddy", "Dz0", "gsend",
-    "intra0", "Dyz0", "Uz-1", "Uz1", "Uyz1", "Ddo", "Uyz-1", "Udz0,0", "st0",
-    "intra1", "Dz1", "Dz-1", "Uz-2", "Ups1", "Udo", "Uz2", "Udz0,1", "st1",
-    "Ddz0,1", "Udz1,0", "Dyz-1", "Uyz-2", "comb", "Ddz0,2", "cell0", "Dyz1", "Udz0,-1",
-    "Uz-3", "Udz-1,0", "Um1", "cell1", "Uz3", "wpass", "Udz0,2", "Udz-1,1", "Udm0",
-    "Udz1,1", "Ups-1", "Uyz3", "Dps-1", "Dz-2", "Udz-1,-1", "Ddz0,-1", "Uyz-3", "Ddm0",
-    "ul0", "Udz2,0", "Ddz1,0", "Ddz1,1", "ur0", "Uyz0", "Uyz2", "Uz-4", "Udz-2,0",
-    "Udz1,2", "ul1", "ur1", "Udz1,-1", "Udz-1,2", "Ddz1,2", "Udm-1", "Dps1", "out0",
-    "Ups3", "Udz3,0", "Uyz-4", "Ddz1,-1", "Udz2,1", "Dyz-2", "out1", "Udz-2,-1", "Ups2",
-    "Udz-2,1", "Dm-1", "Udz2,2", "Ups-3", "Ups0", "Udz2,-1", "Udz-3,0", "Dz2", "Udz-2,2",
-    "Dyz2", "Udz3,1", "Ups-4", "Udz3,2", "Ups-2", "Ddz2,1", "Udm-2", "Ddz2,-1", "Dps0",
-    "Ddz2,2", "fl0", "Dm1", "Udz-3,-1", "Dz-3", "Ddz-1,-1", "Ddz-1,0", "fr0", "Ddz2,0",
-    "Ddz-1,2", "Ddz-1,1", "Udm2", "Um0", "Udz3,-1", "Um-1", "Udm3", "Um3", "Udz-3,1",
-    "Ddm2", "Dps-2", "Udm1", "Um2", "Ddm1", "Dps2", "Dyz-3", "Um-3", "Um-4",
-    "Udz-3,2", "Ddm-1", "Udz-4,0", "Udz-4,-1", "Dz3", "Udm-3", "Dyz3", "fl1", "Udz4,1",
-    "Um-2", "Udz4,2", "Udm4", "Ddz3,1", "fr1", "Dz-4", "Dyz-4", "Ddz3,-1", "Dps-3",
-    "norm0", "Ddz-2,0", "up0,0", "Ddz-2,2", "Ddz-2,-1", "Dm0", "Ddz3,0", "up0,1", "Ddz3,2",
-    "Ddm3", "Dps3", "Ddz-2,1", "up0,2", "Ddm-2", "Dm-2", "up0,3", "Ddz4,1", "s0,0",
-    "Dm2", "Ddz-3,0", "Dps-4", "norm1", "up1,0", "up1,1", "Ddz4,2", "Ddz-3,-1", "Ddz-3,2",
-    "s0,1", "Dm-3", "Ddz-3,1", "up1,2", "Ddm-3", "up1,3", "Ddz-4,0", "Dm3", "s1,0",
-    "Ddz-4,-1", "Ddm4", "Dm-4", "s1,1", "s0,2", "j0,1", "s1,2", "s0,3", "j0,0",
+    "tell", "begin", "Uz0", "Udy", "Uyz0", "Ddz0,0", "intra0", "wsend", "Ddy",
+    "Dz0", "Uz-1", "Uz1", "Uyz-1", "Dyz0", "Uyz1", "Udz0,1", "Udz0,0", "Ddz1,0",
+    "st0", "intra1", "Ups-1", "gsend", "Uz2", "Uz-2", "Dz-1", "st1", "Udo",
+    "Ddo", "Udz0,-1", "Dz1", "Uyz-2", "comb", "cell0", "Uyz2", "wpass", "Dyz-1",
+    "Uz-3", "Udz1,0", "Um-1", "Ddz0,-1", "Ups1", "Ddz0,1", "cell1", "Udz1,1", "Udz-1,-1",
+    "Udz-1,0", "Udz0,2", "Dz2", "Uz3", "ur0", "Ups0", "Udz-1,1", "Ddz0,2", "ul0",
+    "Uz-4", "Uyz-4", "Dyz2", "ul1", "Dps-1", "ur1", "Dz-2", "Ddz1,-1", "Uyz3",
+    "Udz1,-1", "Uyz-3", "Ddz1,1", "Udm0", "Ups2", "Udz-2,-1", "Ddz-1,-1", "Ups-2", "out0",
+    "Ddm0", "Udz1,2", "Udz2,1", "Dyz-2", "out1", "Udz2,0", "Um1", "Um0", "Udz-1,2",
+    "Dz3", "Ups-4", "Udm-1", "Dm-1", "Udz-2,0", "Dyz1", "Udm1", "Dps0", "Ups-3",
+    "Udz2,2", "Udz-2,1", "Udz-3,-1", "fr0", "Dps2", "Um2", "Udz-2,2", "Ups3", "Udz2,-1",
+    "Udz3,1", "Dps1", "Um-3", "Udz-3,0", "fl0", "Udz3,2", "Ddz-1,0", "Dz-3", "Ddz-1,1",
+    "Udm2", "Ddz-1,2", "Ddz1,2", "Dps-2", "Ddz2,1", "Udz3,-1", "Udz3,0", "Udm-2", "Udm3",
+    "Udz-3,1", "Dyz3", "Um3", "Ddz2,-1", "Um-2", "Ddz2,0", "Udz-4,-1", "Udz-3,2", "Udm-3",
+    "fr1", "fl1", "Ddm1", "Dyz-3", "Um-4", "Udz-4,0", "Ddz-2,-1", "Udz4,2", "Udz4,1",
+    "Udm4", "Ddz-2,0", "Ddz2,2", "Ddm2", "norm0", "Dps3", "Ddm-1", "up0,0", "Dm0",
+    "up0,1", "Ddz-2,1", "Ddz3,0", "Ddz3,1", "Dz-4", "Dyz-4", "Ddz3,-1", "norm1", "Dm1",
+    "up0,2", "Dm2", "Dps-3", "Ddz-2,2", "Ddm-2", "Ddz3,2", "up0,3", "s0,0", "Ddz-3,0",
+    "Ddz-3,-1", "Ddz4,1", "Ddz-3,1", "Dm-2", "up1,0", "up1,1", "Dps-4", "Ddz4,2", "Ddz-3,2",
+    "s0,1", "Ddm3", "Ddm-3", "up1,2", "Ddz-4,-1", "Ddz-4,0", "Dm3", "up1,3", "Dm-3",
+    "Ddm4", "s1,0", "Dm-4", "s1,1", "s0,2", "j0,1", "s1,2", "s0,3", "j0,0",
     "s1,3", "j1,0", "j0,2", "j1,2", "j1,1", "j0,3", "j1,3", "sent", "fin0",
     "fin1", "rest",
 )

time: 86 us -> 85.5 us (level)
  the two profiles are of different devices: /device:TPU:1 before, /device:TPU:18 now
where the time goes in v6:
time: 85.5 us; the launch traced here: 85.4 us
  Pallas kernels  83.5 us (98%)
  local copies, waits for them, and re-layouts  1.87 us (2%)
    pallas_call x1, Pallas kernels, layer(): pl.pallas_call(kernel, out_shape=jax.ShapeDtypeStruct((ROWS, OWN), BF16),...  83.5 us
    unnamed x1, local copies, waits for them, and re-layouts  1.87 us

profile of v6, /device:TPU:18, one launch (start us, length us, event | category | flops | bytes accessed | tf_op | source)
XLA Modules:
  0.0 85.4 jit_solution(11849640912760276156)
XLA Ops:
  0.0 83.5 %shard_map.136 = bf16[512,512]{1,0:T(8,128)(2,1)} custom-call(f32[2,512]{1,0:T(2,128)} %bitcast.6, f32[2,512]{1,0:T(2,128)} %bitcast.7, f32[2,512]{1,0:T(2,128)} %bitcast.8, s32[1,512]{1,0:T(1,128)} %bitcast.9, bf16[256]{0:T(256)(128)(2,1)} %cg_h.1, bf16[512]{0:T(512)(128)(2,1)} %mg_h.1, bf16[512,256]{1,0:T(8,128)(2,1)} %q_h.1, bf16[512,256]{1,0:T(8,128)(2,1)} %k_h.1, ...), custom_call_target="tpu_custom_call" | custom-call | tf_op jit(solution)/shard_map/pallas_call | solution.py:588
  83.5 1.9 %copy.16 = bf16[512,512]{1,0:T(8,128)(2,1)} copy(bf16[512,512]{1,0:T(8,128)(2,1)} %shard_map.136) | data formatting | bytes 1048576

commit v7 on v6

--- a/solution.py
+++ b/solution.py
@@ -23,31 +23,31 @@
 RIGHT = {"U": (0, -2, 2, -4), "D": (0, -2, 2)}
 SPLIT = {"U": 16, "D": 24}
 
-RECEIVES = 164
+RECEIVES = 163
 
 ORDER = (
-    "tell", "begin", "Uz0", "Udy", "Uyz0", "Ddz0,0", "intra0", "wsend", "Ddy",
-    "Dz0", "Uz-1", "Uz1", "Uyz-1", "Dyz0", "Uyz1", "Udz0,1", "Udz0,0", "Ddz1,0",
-    "st0", "intra1", "Ups-1", "gsend", "Uz2", "Uz-2", "Dz-1", "st1", "Udo",
-    "Ddo", "Udz0,-1", "Dz1", "Uyz-2", "comb", "cell0", "Uyz2", "wpass", "Dyz-1",
-    "Uz-3", "Udz1,0", "Um-1", "Ddz0,-1", "Ups1", "Ddz0,1", "cell1", "Udz1,1", "Udz-1,-1",
-    "Udz-1,0", "Udz0,2", "Dz2", "Uz3", "ur0", "Ups0", "Udz-1,1", "Ddz0,2", "ul0",
-    "Uz-4", "Uyz-4", "Dyz2", "ul1", "Dps-1", "ur1", "Dz-2", "Ddz1,-1", "Uyz3",
-    "Udz1,-1", "Uyz-3", "Ddz1,1", "Udm0", "Ups2", "Udz-2,-1", "Ddz-1,-1", "Ups-2", "out0",
-    "Ddm0", "Udz1,2", "Udz2,1", "Dyz-2", "out1", "Udz2,0", "Um1", "Um0", "Udz-1,2",
-    "Dz3", "Ups-4", "Udm-1", "Dm-1", "Udz-2,0", "Dyz1", "Udm1", "Dps0", "Ups-3",
-    "Udz2,2", "Udz-2,1", "Udz-3,-1", "fr0", "Dps2", "Um2", "Udz-2,2", "Ups3", "Udz2,-1",
-    "Udz3,1", "Dps1", "Um-3", "Udz-3,0", "fl0", "Udz3,2", "Ddz-1,0", "Dz-3", "Ddz-1,1",
-    "Udm2", "Ddz-1,2", "Ddz1,2", "Dps-2", "Ddz2,1", "Udz3,-1", "Udz3,0", "Udm-2", "Udm3",
-    "Udz-3,1", "Dyz3", "Um3", "Ddz2,-1", "Um-2", "Ddz2,0", "Udz-4,-1", "Udz-3,2", "Udm-3",
-    "fr1", "fl1", "Ddm1", "Dyz-3", "Um-4", "Udz-4,0", "Ddz-2,-1", "Udz4,2", "Udz4,1",
-    "Udm4", "Ddz-2,0", "Ddz2,2", "Ddm2", "norm0", "Dps3", "Ddm-1", "up0,0", "Dm0",
-    "up0,1", "Ddz-2,1", "Ddz3,0", "Ddz3,1", "Dz-4", "Dyz-4", "Ddz3,-1", "norm1", "Dm1",
-    "up0,2", "Dm2", "Dps-3", "Ddz-2,2", "Ddm-2", "Ddz3,2", "up0,3", "s0,0", "Ddz-3,0",
-    "Ddz-3,-1", "Ddz4,1", "Ddz-3,1", "Dm-2", "up1,0", "up1,1", "Dps-4", "Ddz4,2", "Ddz-3,2",
-    "s0,1", "Ddm3", "Ddm-3", "up1,2", "Ddz-4,-1", "Ddz-4,0", "Dm3", "up1,3", "Dm-3",
-    "Ddm4", "s1,0", "Dm-4", "s1,1", "s0,2", "j0,1", "s1,2", "s0,3", "j0,0",
-    "s1,3", "j1,0", "j0,2", "j1,2", "j1,1", "j0,3", "j1,3", "sent", "fin0",
+    "tell", "begin", "Uz0", "Udy", "Ddy", "Dyz0", "intra0", "Ddz0,0", "intra1",
+    "Uyz0", "Dz0", "wsend", "Uz1", "Uz-1", "Ddo", "Uyz1", "Uyz-1", "Ddz1,0",
+    "gsend", "Udz0,1", "st0", "Dz1", "Dz-1", "Uz-2", "Ddz0,1", "Ddz-1,0", "Uz2",
+    "Udo", "Dyz1", "st1", "comb", "Udz1,1", "Ups1", "cell0", "Ddz0,-1", "Uyz2",
+    "Dyz-1", "cell1", "Dz-2", "Ddz2,0", "Ddz0,2", "Uz-3", "Dps1", "Ddz1,1", "Ddm0",
+    "Um1", "Udz0,-1", "Ups-1", "Uyz-2", "Ddz-1,-1", "Uyz-3", "ul0", "ur0", "Uz3",
+    "Udz0,2", "Ddz1,-1", "Udz0,0", "Dz-3", "ul1", "Uz-4", "Dps-1", "Uyz-4", "Uyz3",
+    "Dz2", "ur1", "Udm0", "wpass", "Udz1,-1", "out0", "Ups0", "Ddz3,0", "Ups2",
+    "Udz1,2", "Udz-1,-1", "Dps0", "Udz1,0", "Dm1", "Udz-1,0", "Ups-2", "Ddz1,2", "Dyz-3",
+    "Udz-1,2", "Udm1", "Udz-1,1", "Dz3", "out1", "Dz-4", "Udz2,1", "Ups-3", "Ups-4",
+    "Udz-2,-1", "Dm-1", "Udz2,2", "Um-1", "Um0", "Udz2,0", "Dyz-4", "Ups3", "Udz-2,0",
+    "Ddz2,-1", "Dyz3", "Udz2,-1", "Ddm1", "fr0", "fl0", "Ddz2,2", "Um2", "Udz-2,2",
+    "Udz-2,1", "Udz3,1", "Udz-3,-1", "Udz3,2", "Ddz2,1", "Udz-3,0", "Ddz-1,1", "Udm-1", "Udz3,0",
+    "Ddz-1,2", "Udm2", "Udm-2", "Ddm2", "Um-3", "Udz-3,2", "fr1", "Dps-4", "fl1",
+    "Ddz-2,-1", "Dm0", "Ddm-1", "Dps-3", "Um-2", "Um3", "Ddz3,-1", "Udz3,-1", "Udm3",
+    "Udz4,1", "Dps3", "Udz-4,-1", "Um-4", "Ddz-2,0", "Dyz-2", "Udz-3,1", "Dyz2", "Udm-3",
+    "Ddz3,2", "Udz4,2", "Udz-4,0", "Udm4", "norm0", "Ddz-2,1", "Ddz-2,2", "up0,0", "Ddz-3,-1",
+    "norm1", "Ddz3,1", "Ddm3", "Ddz-3,0", "up1,0", "Dm-3", "Dm-4", "Dps-2", "Ddz4,2",
+    "up0,1", "Ddz-3,1", "Ddm-2", "up0,2", "Dm3", "Ddz-3,2", "Ddm-3", "up0,3", "Dps2",
+    "Ddz-4,-1", "Ddz-4,0", "Ddz4,1", "Ddm4", "up1,1", "s0,0", "up1,2", "Dm-2", "s0,1",
+    "Dm2", "up1,3", "s1,0", "s1,1", "s0,2", "s0,3", "s1,2", "s1,3", "j0,0",
+    "j0,2", "j0,3", "j1,0", "j1,2", "j0,1", "j1,1", "j1,3", "sent", "fin0",
     "fin1", "rest",
 )
 
@@ -160,7 +160,7 @@
         def come(*names):
             arrived(*(w + name for name in names))
 
-        mates = lambda zo: "U" if w == "U" else "D%d" % max(abs(zo) - 1, 0)
+        mates = lambda zo: "U" if w == "U" else "D%d" % (0, 0, 2, 1, 1)[abs(zo)]
 
         def along_z(zo):
             if zo:
@@ -496,7 +496,7 @@
         steps["up1,%d" % t] = lambda t=t: up(1, t)
 
     zb = lax.rem(z, 2)
-    owner = [lax.rem(z // 2 + d + NX, NX) for d in (0, 2 * zb - 1, 1 - 2 * zb, 2)]
+    owner = [lax.rem(z // 2 + d + NX, NX) for d in (0, 2, 2 * zb - 1, 1 - 2 * zb)]
     ahead_by = [lax.rem(o - x + NX, NX) for o in owner]
     ways = ((0, xr), (1, xl), (1, xr), (0, xl), (0, xr), (1, xl))
     quarter = lambda s, h: slice(256 * s + 128 * h, 256 * s + 128 * h + 128)
@@ -510,7 +510,8 @@
 
     def stage(s, k):
         if s == 0:
-            all_arrived("D%d" % k, (wdn.at[0:3, :, 0], wdn.at[0], wdn.at[0], wdn.at[0, :, 0])[k])
+            if k < 3:
+                all_arrived("D%d" % k, (wdn.at[0:3, :, 0], wdn.at[0:3, :, 0], wdn.at[0])[k])
         w = wdn[pl.ds(2 * owner[k], 2)].reshape(OWN, DM)
         rows = slice(256 * s, 256 * s + 256)
         terms[k, rows] = lax.dot_general(
@@ -548,7 +549,7 @@
     def final(s):
         d = lax.rem(x - z // 2 + NX, NX)
         d = lax.rem(d * (2 * zb - 1) + NX, NX)
-        mine = terms.at[d + d // 2 - 2 * (d // 3)]
+        mine = terms.at[2 * lax.rem(d, 2) + d // 2]
         for h, i, n in ((0, 3, 4), (1, 2, 5)):
             part(s, i, 0).wait_recv()
             part(s, n, 0).wait_recv()

time: 85.5 us -> 85 us (level)
  the two profiles are of different devices: /device:TPU:18 before, /device:TPU:1 now
where the time goes in v7:
time: 85 us; the launch traced here: 84.8 us
  Pallas kernels  82.9 us (98%)
  local copies, waits for them, and re-layouts  1.87 us (2%)
    pallas_call x1, Pallas kernels, layer(): pl.pallas_call(kernel, out_shape=jax.ShapeDtypeStruct((ROWS, OWN), BF16),...  82.9 us
    unnamed x1, local copies, waits for them, and re-layouts  1.87 us

profile of v7, /device:TPU:1, one launch (start us, length us, event | category | flops | bytes accessed | tf_op | source)
XLA Modules:
  0.0 84.8 jit_solution(5258068273887784513)
XLA Ops:
  0.0 82.9 %shard_map.136 = bf16[512,512]{1,0:T(8,128)(2,1)} custom-call(f32[2,512]{1,0:T(2,128)} %bitcast.6, f32[2,512]{1,0:T(2,128)} %bitcast.7, f32[2,512]{1,0:T(2,128)} %bitcast.8, s32[1,512]{1,0:T(1,128)} %bitcast.9, bf16[256]{0:T(256)(128)(2,1)} %cg_h.1, bf16[512]{0:T(512)(128)(2,1)} %mg_h.1, bf16[512,256]{1,0:T(8,128)(2,1)} %q_h.1, bf16[512,256]{1,0:T(8,128)(2,1)} %k_h.1, ...), custom_call_target="tpu_custom_call" | custom-call | tf_op jit(solution)/shard_map/pallas_call | solution.py:589
  83.0 1.9 %copy.16 = bf16[512,512]{1,0:T(8,128)(2,1)} copy(bf16[512,512]{1,0:T(8,128)(2,1)} %shard_map.136) | data formatting | bytes 1048576
